TPU v7x, 32 devices: a whole 2x2x4 slice. The times are simulated.
32 devices in a mesh: ep: 8 (over z, y), tp: 4 (over x, core).
Axes of the slice: x: 2, y: 2, z: 4, core: 2. Of those that a mesh axis runs over, the one named last changes fastest.
Arguments:
- tokens: bfloat16 [2560, 2048], P('ep'), may hold values from -12 to 12, as said below
- cotangent: bfloat16 [2560, 2048], P('ep'), may hold values from -0.59765625 to 0.59765625
- route_ids: int32 [2560, 2], P('ep'), may hold values from 0 to 7, all different within a row; in each aligned block of 320 rows (0 to 319, 320 to 639, ...) at most 160 rows name the same one
- route_weights: bfloat16 [2560, 2], P('ep'), may hold values from 0.049804688 to 1
- w_gate: bfloat16 [8, 2048, 2048], P('ep', None, 'tp'), may hold values from -0.125 to 0.125
- w_up: bfloat16 [8, 2048, 2048], P('ep', None, 'tp'), may hold values from -0.125 to 0.125
- w_down: bfloat16 [8, 2048, 2048], P('ep', 'tp'), may hold values from -0.125 to 0.125
- dense_in: bfloat16 [2048, 256], P(('ep', 'tp')), may hold values from -0.125 to 0.125
- dense_out: bfloat16 [2048, 256], P(('ep', 'tp')), may hold values from -0.375 to 0.375
- dense_gate: bfloat16 [2048], replicated, may hold values from -0.125 to 0.125
Outputs:
- grad_tokens: bfloat16 [2560, 2048], P('ep', 'tp')
- grad_route_weights: bfloat16 [2560, 2], P('ep')
- grad_gate: float32 [8, 2048, 2048], P('ep', None, 'tp')
- grad_up: float32 [8, 2048, 2048], P('ep', None, 'tp')
- grad_down: float32 [8, 2048, 2048], P('ep', 'tp')
- grad_dense_in: float32 [2048, 256], P(('ep', 'tp'))
- grad_dense_out: float32 [2048, 256], P(('ep', 'tp'))
- grad_dense_gate: float32 [2048], P(('ep', 'tp'))
Inputs may be any that keep to these rules, and one draw needn't show every extreme that they name: `route_ids`: each row names 2 different experts; among the rows of one index of ep no expert is named more than 160 times, and that count is reached. `tokens`: rows carry scales between 0.5 and 2 that differ from row to row.
All inputs are finite; a program needn't handle non-finite values.
Results may differ from a plain program's by a relative error of at most 0.01.
Values may be sent and summed in bfloat16 or wider, within the bound.
A program may use at most 128 MiB of HBM per device.

v0:
```python
import functools

import jax
import jax.numpy as jnp
from jax import lax
from jax.experimental import pallas as pl
from jax.experimental.pallas import tpu as pltpu
from jax.sharding import PartitionSpec as P

CLAMP_LIMIT = 7.0
SIG_SLOPE = 1.702
MESH = pl.DeviceIdType.MESH
ANY = pl.BlockSpec(memory_space=pl.ANY)
VMEM = pl.BlockSpec(memory_space=pltpu.VMEM)


def greet(devices):
    barrier = pltpu.get_barrier_semaphore()
    for device in devices:
        pl.semaphore_signal(barrier, inc=1, device_id=device, device_id_type=MESH)
    pl.semaphore_wait(barrier, len(devices))


def dispatch_kernel(
    n_ep,
    x_quarter,
    dy_quarter,
    x_own,
    dy_own,
    weight_rows,
    in_own,
    out_own,
    gate_w,
    up_w,
    down_w,
    x_out,
    scaled_out,
    act_out,
    dgate_out,
    dup_out,
    part_out,
    weight_part,
    in_all,
    out_all,
    x_all,
    scaled_all,
    act_all,
    dgate_all,
    dup_all,
    part_all,
    dy_all,
    weight_all,
    shard_buf,
    local_sem,
    out_sem,
    send_rows,
    recv_rows,
    send_shard,
    recv_shard,
    send_w,
    recv_w,
):
    me = lax.axis_index("ep")
    t = lax.axis_index("tp")
    half = t // 2
    side = t % 2
    t_core = half * 2 + 1 - side
    t_x = (1 - half) * 2 + side
    cap, cols = x_quarter.shape[1:]
    lanes = weight_rows.shape[2]
    f32 = jnp.float32
    bf = jnp.bfloat16

    def ahead(k):
        return lax.rem(me + k, n_ep)

    def behind(k):
        return lax.rem(me + n_ep - k, n_ep)

    def offset(n):
        return n_ep // 2 + (n // 2) * (1 - 2 * (n % 2))

    core_peer = (me, t_core)
    x_peer = (me, t_x)
    greet([(ahead(k), t) for k in range(1, n_ep)] + [core_peer, x_peer])

    rows_in = (x_quarter, dy_quarter)
    rows_out = (x_all, dy_all)
    shards_in = (in_own, out_own)
    shards_out = (in_all, out_all)

    def row_slice(a, i, q):
        return rows_out[a].at[i, :, pl.ds(pl.multiple_of(q * cols, cols), cols)]

    def copy_to(src, dst, send, recv, device):
        return pltpu.make_async_remote_copy(
            src_ref=src,
            dst_ref=dst,
            send_sem=send,
            recv_sem=recv,
            device_id=device,
            device_id_type=MESH,
        )

    def shard_hop(a, kind, k, first=False):
        i = behind(k)
        sems = (send_shard.at[a, kind, k], recv_shard.at[a, kind, k])
        if kind == 0:
            return copy_to(shards_in[a], shards_out[a].at[me, t], *sems, (ahead(k), t))
        if kind == 3:
            block = shards_out[a].at[i, t_x]
            return copy_to(block, block, *sems, core_peer)
        block = shards_out[a].at[i, t]
        return copy_to(
            shards_in[a] if first else block, block, *sems, x_peer if kind == 1 else core_peer
        )

    def row_hop(a, kind, k):
        i = behind(k)
        sems = (send_rows.at[a, kind, k], recv_rows.at[a, kind, k])
        if kind == 0:
            return copy_to(rows_in[a].at[ahead(k)], row_slice(a, me, t), *sems, (ahead(k), t))
        block = row_slice(a, i, t_x if kind == 3 else t)
        return copy_to(block, block, *sems, x_peer if kind == 1 else core_peer)

    def w_hop(k):
        return copy_to(
            weight_rows.at[ahead(k)], weight_all.at[me], send_w.at[k], recv_w.at[k], (ahead(k), t)
        )

    for a in range(2):
        shard_hop(a, 1, 0, True).start()
        shard_hop(a, 2, 0, True).start()

    @pl.loop(1, n_ep)
    def _(n):
        k = offset(n)
        for a in range(2):
            shard_hop(a, 0, k).start()
        w_hop(k).start()
        for a in range(2):
            row_hop(a, 0, k).start()

    ins = [
        pltpu.make_async_copy(in_own, shard_buf.at[0], local_sem.at[0]),
        pltpu.make_async_copy(out_own, shard_buf.at[1], local_sem.at[1]),
        pltpu.make_async_copy(x_own, x_all.at[me], local_sem.at[2]),
        pltpu.make_async_copy(dy_own, dy_all.at[me], local_sem.at[3]),
    ]
    outs = [
        pltpu.make_async_copy(shard_buf.at[0], in_all.at[me, t], local_sem.at[4]),
        pltpu.make_async_copy(shard_buf.at[1], out_all.at[me, t], local_sem.at[5]),
    ]
    for c in ins:
        c.start()
    weight_all[pl.ds(me, 1)] = weight_rows[pl.ds(me, 1)]
    for c in ins:
        c.wait()
    for c in outs:
        c.start()

    diagonal = lax.broadcasted_iota(jnp.int32, (cap, lanes), 0) == lax.broadcasted_iota(
        jnp.int32, (cap, lanes), 1
    )
    contract_cols = (((1,), (1,)), ((), ()))

    def compute(i):
        weight_row = weight_all[i, 0:1].astype(f32)
        route_col = jnp.sum(jnp.where(diagonal, weight_row, 0.0), axis=1, keepdims=True)
        x_rows = x_all[i]
        gate_pre = jnp.dot(x_rows, gate_w[...], preferred_element_type=f32)
        up_pre = jnp.dot(x_rows, up_w[...], preferred_element_type=f32)
        gate_clamp = jnp.minimum(gate_pre, CLAMP_LIMIT)
        up_clamp = jnp.clip(up_pre, -CLAMP_LIMIT, CLAMP_LIMIT)
        sig = jax.nn.sigmoid(SIG_SLOPE * gate_clamp)
        act = (gate_clamp * sig * (up_clamp + 1.0)).astype(bf)
        act_all[i] = act
        dy_rows = dy_all[i]
        scaled_all[i] = (route_col * dy_rows.astype(f32)).astype(bf)
        back = lax.dot_general(
            dy_rows, down_w[...], contract_cols, preferred_element_type=f32
        )
        weight_sum = jnp.sum(act.astype(f32) * back, axis=1, keepdims=True)
        weight_lane = jnp.sum(jnp.where(diagonal, weight_sum, 0.0), axis=0, keepdims=True)
        weight_part[i] = jnp.broadcast_to(weight_lane, (8, lanes))
        d_act = route_col * back
        d_gate = jnp.where(
            gate_pre < CLAMP_LIMIT,
            d_act * (up_clamp + 1.0) * (sig + SIG_SLOPE * gate_clamp * sig * (1.0 - sig)),
            0.0,
        ).astype(bf)
        d_up = jnp.where(jnp.abs(up_pre) < CLAMP_LIMIT, d_act * gate_clamp * sig, 0.0).astype(bf)
        dgate_all[i] = d_gate
        dup_all[i] = d_up
        part = lax.dot_general(d_gate, gate_w[...], contract_cols, preferred_element_type=f32)
        part = part + lax.dot_general(d_up, up_w[...], contract_cols, preferred_element_type=f32)
        part_all[i] = part.astype(bf)

    results = (
        (x_all, x_out),
        (part_all, part_out),
        (scaled_all, scaled_out),
        (act_all, act_out),
        (dgate_all, dgate_out),
        (dup_all, dup_out),
    )

    def store(i):
        return [
            pltpu.make_async_copy(src.at[i], dst.at[i], out_sem.at[a, i])
            for a, (src, dst) in enumerate(results)
        ]

    @pl.loop(0, n_ep + 2)
    def _(n):
        @pl.when((n >= 1) & (n < n_ep))
        def _():
            k = offset(n)
            for a in range(2):
                shard_hop(a, 0, k).wait_recv()
                shard_hop(a, 1, k).start()
                shard_hop(a, 2, k).start()
            for a in range(2):
                row_hop(a, 0, k).wait_recv()
                row_hop(a, 1, k).start()
                row_hop(a, 2, k).start()

        @pl.when((n >= 1) & (n < n_ep + 1))
        def _():
            k = jnp.where(n == 1, 0, offset(jnp.maximum(n - 1, 1)))
            for a in range(2):
                shard_hop(a, 1, k).wait_recv()
                shard_hop(a, 3, k).start()

        @pl.when((n >= 2) & (n < n_ep + 1))
        def _():
            k = offset(n - 1)
            for a in range(2):
                row_hop(a, 1, k).wait_recv()
                row_hop(a, 3, k).start()

        @pl.when(n >= 3)
        def _():
            k = offset(n - 2)
            w_hop(k).wait_recv()
            for a in range(2):
                for kind in (2, 3):
                    row_hop(a, kind, k).wait_recv()

        @pl.when((n == 0) | (n >= 3))
        def _():
            i = behind(jnp.where(n == 0, 0, offset(jnp.maximum(n - 2, 1))))
            compute(i)
            for c in store(i):
                c.start()

    @pl.loop(0, n_ep)
    def _(k):
        for a in range(2):
            for kind in (2, 3):
                shard_hop(a, kind, k).wait_recv()
            for kind in (1, 2, 3):
                shard_hop(a, kind, k).wait_send()
        for c in store(k):
            c.wait()

    @pl.loop(1, n_ep)
    def _(k):
        for a in range(2):
            shard_hop(a, 0, k).wait_send()
            for kind in range(4):
                row_hop(a, kind, k).wait_send()
        w_hop(k).wait_send()

    for c in outs:
        c.wait()


def return_kernel(
    n_ep,
    n_tp,
    part,
    grad_in,
    grad_out,
    grad_gate,
    weight_part,
    rows_back,
    in_back,
    out_back,
    gate_back,
    weight_back,
    from_core,
    to_x,
    from_x,
    to_ep,
    send_core,
    recv_core,
    send_x,
    recv_x,
    send_ep,
    recv_ep,
    send_grad,
    recv_grad,
    send_w,
    recv_w,
):
    me = lax.axis_index("ep")
    t = lax.axis_index("tp")
    half = t // 2
    side = t % 2
    t_core = half * 2 + 1 - side
    t_x = (1 - half) * 2 + side
    cols = rows_back.shape[2]

    def ahead(k):
        return lax.rem(me + k, n_ep)

    def quarter(q):
        return pl.ds(pl.multiple_of(q * cols, cols), cols)

    core_peer = (me, t_core)
    x_peer = (me, t_x)
    others = [
        (ahead(k), lax.rem(t + d, n_tp))
        for k in range(n_ep)
        for d in range(n_tp)
        if k > 0 or d > 0
    ]
    greet(others)

    def copy_to(src, dst, send, recv, device):
        return pltpu.make_async_remote_copy(
            src_ref=src,
            dst_ref=dst,
            send_sem=send,
            recv_sem=recv,
            device_id=device,
            device_id_type=MESH,
        )

    started = []

    def go(copy):
        copy.start()
        started.append(copy)

    order = list(range(1, n_ep)) + [0]

    def core_hop(k, h):
        j = ahead(k)
        return copy_to(
            part.at[j, :, quarter(h * 2 + 1 - side)],
            from_core.at[k, h],
            send_core.at[k, h],
            recv_core.at[k, h],
            core_peer,
        )

    def x_hop(k):
        return copy_to(to_x.at[k], from_x.at[k], send_x.at[k], recv_x.at[k], x_peer)

    def ep_hop(k):
        return copy_to(
            to_ep.at[k], rows_back.at[me], send_ep.at[k], recv_ep.at[k], (ahead(k), t)
        )

    for k in order:
        for h in range(2):
            go(core_hop(k, h))
    grads = ((grad_in, in_back), (grad_out, out_back), (grad_gate, gate_back))

    def grad_hop(a, k):
        src, dst = grads[a]
        return copy_to(
            src.at[ahead(k)],
            dst.at[me],
            send_grad.at[a, k],
            recv_grad.at[a, k],
            (ahead(k), t),
        )

    def w_hop(k, d):
        return copy_to(
            weight_part.at[ahead(k)],
            weight_back.at[me, t],
            send_w.at[k, d],
            recv_w.at[k, d],
            (ahead(k), lax.rem(t + d, n_tp)),
        )

    for k in range(n_ep):
        for d in range(n_tp):
            if k > 0 or d > 0:
                go(w_hop(k, d))
        if k > 0:
            for a in range(3):
                go(grad_hop(a, k))
    for a in range(3):
        grads[a][1][pl.ds(me, 1)] = grads[a][0][pl.ds(me, 1)]
    weight_back[pl.ds(me, 1), pl.ds(t, 1)] = weight_part[pl.ds(me, 1)][:, None]

    def finish(k):
        j = ahead(k)
        x_hop(k).wait_recv()
        mine = part[j, :, quarter(t)].astype(jnp.float32)
        mine = mine + from_core[k, half].astype(jnp.float32)
        mine = (mine + from_x[k].astype(jnp.float32)).astype(jnp.bfloat16)
        if k > 0:
            to_ep[k] = mine
            go(ep_hop(k))
        else:
            rows_back[me] = mine

    lag = 2
    for n, k in enumerate(order):
        j = ahead(k)
        for h in range(2):
            core_hop(k, h).wait_recv()
        other = part[j, :, quarter(t_x)].astype(jnp.float32)
        other = other + from_core[k, 1 - half].astype(jnp.float32)
        to_x[k] = other.astype(jnp.bfloat16)
        go(x_hop(k))
        if n >= lag:
            finish(order[n - lag])
    for k in order[n_ep - lag :]:
        finish(k)

    for k in range(n_ep):
        if k > 0:
            ep_hop(k).wait_recv()
            for a in range(3):
                grad_hop(a, k).wait_recv()
        for d in range(n_tp):
            if k > 0 or d > 0:
                w_hop(k, d).wait_recv()
    for c in started:
        c.wait_send()


def dispatch(n_ep, n_tp, *args):
    x_quarter, _, x_own, _, weight_rows, in_own, _, gate_w, _, _ = args
    cap, cols = x_quarter.shape[1:]
    width = x_own.shape[1]
    hidden = gate_w.shape[1]
    lanes = weight_rows.shape[2]
    bf = jnp.bfloat16
    dma = pltpu.SemaphoreType.DMA
    rows = jax.ShapeDtypeStruct((n_ep, cap, width), bf)
    inner = jax.ShapeDtypeStruct((n_ep, cap, hidden), bf)
    shard = jax.ShapeDtypeStruct((n_ep, n_tp) + in_own.shape, bf)
    return pl.pallas_call(
        functools.partial(dispatch_kernel, n_ep),
        out_shape=(
            rows,
            rows,
            inner,
            inner,
            inner,
            rows,
            jax.ShapeDtypeStruct((n_ep, 8, lanes), jnp.float32),
            shard,
            shard,
        ),
        in_specs=[ANY, ANY, ANY, ANY, VMEM, ANY, ANY, VMEM, VMEM, VMEM],
        out_specs=(ANY,) * 6 + (VMEM, ANY, ANY),
        scratch_shapes=[
            pltpu.VMEM(rows.shape, bf),
            pltpu.VMEM(rows.shape, bf),
            pltpu.VMEM(inner.shape, bf),
            pltpu.VMEM(inner.shape, bf),
            pltpu.VMEM(inner.shape, bf),
            pltpu.VMEM(rows.shape, bf),
            pltpu.VMEM(rows.shape, bf),
            pltpu.VMEM(weight_rows.shape, bf),
            pltpu.VMEM((2,) + in_own.shape, bf),
            dma((6,)),
            dma((6, n_ep)),
            dma((2, 4, n_ep)),
            dma((2, 4, n_ep)),
            dma((2, 4, n_ep)),
            dma((2, 4, n_ep)),
            dma((n_ep,)),
            dma((n_ep,)),
        ],
        compiler_params=pltpu.CompilerParams(
            collective_id=0, has_side_effects=True, vmem_limit_bytes=56 * 1024 * 1024
        ),
        name="dispatch",
    )(*args)


def give_back(n_ep, n_tp, *args):
    part, grad_in, grad_out, grad_gate, weight_part = args
    cap, width = part.shape[1:]
    cols = width // n_tp
    bf = jnp.bfloat16
    dma = pltpu.SemaphoreType.DMA
    same = lambda a: jax.ShapeDtypeStruct(a.shape, a.dtype)
    return pl.pallas_call(
        functools.partial(return_kernel, n_ep, n_tp),
        out_shape=(
            jax.ShapeDtypeStruct((n_ep, cap, cols), bf),
            same(grad_in),
            same(grad_out),
            same(grad_gate),
            jax.ShapeDtypeStruct((n_ep, n_tp) + weight_part.shape[1:], weight_part.dtype),
        ),
        in_specs=[VMEM] * 5,
        out_specs=(VMEM,) * 5,
        scratch_shapes=[
            pltpu.VMEM((n_ep, 2, cap, cols), bf),
            pltpu.VMEM((n_ep, cap, cols), bf),
            pltpu.VMEM((n_ep, cap, cols), bf),
            pltpu.VMEM((n_ep, cap, cols), bf),
            dma((n_ep, 2)),
            dma((n_ep, 2)),
            dma((n_ep,)),
            dma((n_ep,)),
            dma((n_ep,)),
            dma((n_ep,)),
            dma((3, n_ep)),
            dma((3, n_ep)),
            dma((n_ep, n_tp)),
            dma((n_ep, n_tp)),
        ],
        compiler_params=pltpu.CompilerParams(
            collective_id=1, has_side_effects=True, vmem_limit_bytes=40 * 1024 * 1024
        ),
        name="give_back",
    )(*args)


def shards(
    tokens,
    cotangent,
    route_ids,
    route_weights,
    w_gate,
    w_up,
    w_down,
    dense_in,
    dense_out,
    dense_gate,
):
    count_ep = lax.axis_size("ep")
    count_tp = lax.axis_size("tp")
    ep_index = lax.axis_index("ep")
    tp_index = lax.axis_index("tp")
    tok_dev, model_width = tokens.shape
    top_k = route_ids.shape[1]
    col_count = model_width // count_tp
    capacity = 2 * tok_dev * top_k // count_ep
    lanes = -(-capacity // 128) * 128
    slot_total = count_ep * capacity
    bf = jnp.bfloat16
    f32 = jnp.float32

    names = jnp.arange(count_ep, dtype=jnp.int32)
    chosen = route_ids[:, :, None] == names[None, None, :]
    member = jnp.any(chosen, axis=1).astype(bf)
    row = jnp.arange(tok_dev, dtype=jnp.int32)
    below = (row[None, :] < row[:, None]).astype(bf)
    rank = jnp.dot(below, member, preferred_element_type=f32)
    slot_index = jnp.sum(jnp.where(chosen, rank[:, None, :], 0.0), axis=2).astype(jnp.int32)
    target = route_ids * capacity + slot_index
    lane_target = route_ids * lanes + slot_index
    slots = jnp.arange(slot_total, dtype=jnp.int32)
    pick = slots[:, None] == target[:, 0][None, :]
    for k in range(1, top_k):
        pick = pick | (slots[:, None] == target[:, k][None, :])
    pick = pick.astype(bf)
    tok_part = lax.dynamic_slice_in_dim(tokens, tp_index * col_count, col_count, 1)
    cot_part = lax.dynamic_slice_in_dim(cotangent, tp_index * col_count, col_count, 1)
    quarter_shape = (count_ep, capacity, col_count)
    x_quarter = jnp.dot(pick, tok_part, preferred_element_type=bf).reshape(quarter_shape)
    dy_quarter = jnp.dot(pick, cot_part, preferred_element_type=bf).reshape(quarter_shape)
    pick_own = lax.dynamic_slice_in_dim(pick, ep_index * capacity, capacity, 0)
    x_own = jnp.dot(pick_own, tokens, preferred_element_type=bf)
    dy_own = jnp.dot(pick_own, cotangent, preferred_element_type=bf)
    lane_slots = jnp.arange(count_ep * lanes, dtype=jnp.int32)
    lane_hits = lane_target[:, :, None] == lane_slots[None, None, :]
    weight_rows = jnp.sum(
        jnp.where(lane_hits, route_weights.astype(f32)[:, :, None], 0.0), axis=(0, 1)
    ).astype(bf)
    weight_rows = jnp.broadcast_to(
        weight_rows.reshape(count_ep, 1, lanes), (count_ep, 16, lanes)
    )
    x_in, scaled_in, act, d_gate, d_up, part, weight_part, in_all, out_all = dispatch(
        count_ep,
        count_tp,
        x_quarter,
        dy_quarter,
        x_own,
        dy_own,
        weight_rows,
        dense_in,
        dense_out,
        w_gate[0],
        w_up[0],
        w_down[0],
    )
    in_whole = in_all.reshape(model_width, -1)
    out_whole = out_all.reshape(model_width, -1)
    x_slots = x_in.reshape(slot_total, model_width)
    scaled_cot = scaled_in.reshape(slot_total, model_width)
    contract_rows = (((0,), (0,)), ((), ()))
    contract_cols = (((1,), (1,)), ((), ()))
    act, d_gate, d_up = (a.reshape(slot_total, -1) for a in (act, d_gate, d_up))
    grad_gate = lax.dot_general(x_slots, d_gate, contract_rows, preferred_element_type=f32)
    grad_up = lax.dot_general(x_slots, d_up, contract_rows, preferred_element_type=f32)
    grad_down = lax.dot_general(act, scaled_cot, contract_rows, preferred_element_type=f32)

    dense_pre = jnp.dot(tokens, in_whole, preferred_element_type=f32)
    dense_act = jax.nn.silu(dense_pre).astype(bf)
    dense_val = lax.dot_general(dense_act, out_whole, contract_cols, preferred_element_type=f32)
    mix = jax.nn.sigmoid(jnp.dot(tokens, dense_gate, preferred_element_type=f32))
    cot_wide = cotangent.astype(f32)
    dense_scaled = (mix[:, None] * cot_wide).astype(bf)
    dense_back = jnp.dot(dense_scaled, out_whole, preferred_element_type=f32)
    sig_pre = jax.nn.sigmoid(dense_pre)
    dense_dpre = (dense_back * sig_pre * (1.0 + dense_pre * (1.0 - sig_pre))).astype(bf)
    dlogit = mix * (1.0 - mix) * jnp.sum(cot_wide * dense_val, axis=1)
    in_rows = lax.dynamic_slice_in_dim(in_whole, tp_index * col_count, col_count, 0)
    gate_cols = lax.dynamic_slice_in_dim(dense_gate, tp_index * col_count, col_count, 0)
    dense_dx = lax.dot_general(dense_dpre, in_rows, contract_cols, preferred_element_type=f32)
    dense_dx = dense_dx + dlogit[:, None] * gate_cols.astype(f32)[None, :]
    block_cols = model_width // (count_ep * count_tp)
    tokens_own = lax.dynamic_index_in_dim(
        tokens.reshape(tok_dev, count_ep, count_tp, block_cols), tp_index, 2, keepdims=False
    ).reshape(tok_dev, count_ep * block_cols)
    scaled_own = lax.dynamic_index_in_dim(
        dense_scaled.reshape(tok_dev, count_ep, count_tp, block_cols), tp_index, 2, keepdims=False
    ).reshape(tok_dev, count_ep * block_cols)
    in_partial = lax.dot_general(tokens_own, dense_dpre, contract_rows, preferred_element_type=f32)
    out_partial = lax.dot_general(scaled_own, dense_act, contract_rows, preferred_element_type=f32)
    gate_partial = jnp.sum(tokens_own.astype(f32) * dlogit[:, None], axis=0)
    gate_partial = jnp.pad(
        gate_partial.reshape(count_ep, 1, block_cols), ((0, 0), (0, 7), (0, -block_cols % 128))
    )

    rows_back, in_back, out_back, gate_back, weight_back = give_back(
        count_ep,
        count_tp,
        part,
        in_partial.astype(bf).reshape(count_ep, block_cols, -1),
        out_partial.astype(bf).reshape(count_ep, block_cols, -1),
        gate_partial,
        weight_part,
    )
    grad_dense_in = jnp.sum(in_back.astype(f32), axis=0)
    grad_dense_out = jnp.sum(out_back.astype(f32), axis=0)
    grad_dense_gate = jnp.sum(gate_back[:, 0, :block_cols], axis=0)
    expert_dx = lax.dot_general(
        pick, rows_back.reshape(slot_total, col_count), contract_rows, preferred_element_type=f32
    )
    grad_tokens = (dense_dx + expert_dx).astype(bf)
    weight_grad = jnp.sum(weight_back[:, :, 0, :], axis=1).reshape(-1)
    grad_route_weights = jnp.sum(
        jnp.where(lane_hits, weight_grad[None, None, :], 0.0), axis=2
    ).astype(bf)
    return (
        grad_tokens,
        grad_route_weights,
        grad_gate[None],
        grad_up[None],
        grad_down[None],
        grad_dense_in,
        grad_dense_out,
        grad_dense_gate,
    )


def solution(mesh):
    placed = (
        P("ep", None),
        P("ep", None),
        P("ep", None),
        P("ep", None),
        P("ep", None, "tp"),
        P("ep", None, "tp"),
        P("ep", "tp", None),
        P(("ep", "tp"), None),
        P(("ep", "tp"), None),
        P(),
    )
    return jax.shard_map(
        shards,
        mesh=mesh,
        in_specs=placed,
        out_specs=(
            P("ep", "tp"),
            P("ep", None),
            P("ep", None, "tp"),
            P("ep", None, "tp"),
            P("ep", "tp", None),
            P(("ep", "tp"), None),
            P(("ep", "tp"), None),
            P(("ep", "tp")),
        ),
        check_vma=False,
    )
```

profile of v0, /device:TPU:12, one launch (start us, length us, event | category | flops | bytes accessed | tf_op | source)
XLA Modules:
  0.0 219.3 jit_solution(14443682918779645805)
XLA Ops:
  0.6 0.8 fusion.16
  1.6 0.8 select_reduce_fusion.2
  2.3 0.7 multiply_add_fusion
  3.1 2.9 %fusion.7 = bf16[1280,512]{1,0:T(8,128)(2,1)} fusion(bf16[320,2048]{1,0:T(8,128)(2,1)} %param.11, s32[]{:T(128)S(6)} %select_n.27, s32[320]{0:T(512)S(1)} %get-tuple-element.37, s32[320]{0:T(512)S(1)} %get-tuple-element.36), kind=kOutput, calls=%fused_computation.30 | convolution fusion | flops 420659200 | bytes 1640964 | tf_op jit(solution)/shard_map/dot_general | solution.py:576
  6.0 1.9 fusion.9
  8.3 1.4 fusion.12.dy_own
  9.7 1.3 fusion.14.x_own
  11.0 0.7 select_reduce_fusion.1
  12.4 117.8 %dispatch.1 = (bf16[8,160,2048]{2,1,0:T(8,128)(2,1)}, bf16[8,160,2048]{2,1,0:T(8,128)(2,1)}, bf16[8,160,512]{2,1,0:T(8,128)(2,1)}, bf16[8,160,512]{2,1,0:T(8,128...) custom-call(bf16[8,160,512]{2,1,0:T(8,128)(2,1)} %bitcast.59, ...), custom_call_target="tpu_custom_call" | custom-call | tf_op jit(solution)/shard_map/dispatch/pallas_call | solution.py:451
  130.3 1.8 convolution_bitcast_fusion.3
  133.3 1.3 fusion
  134.6 1.8 copy.29
  136.9 1.6 copy.28
  138.5 1.2 multiply_reduce_fusion
  139.6 1.8 fusion.5
  141.7 2.5 %copy-done = bf16[8,160,2048]{2,1,0:T(8,128)(2,1)S(1)} copy-done((bf16[8,160,2048]{2,1,0:T(8,128)(2,1)S(1)}, bf16[8,160,2048]{2,1,0:T(8,128)(2,1)}, u32[]{:S(2)}) %copy-start) | copy-done | bytes 5242904
  144.2 53.3 %give_back.1 = (bf16[8,160,512]{2,1,0:T(8,128)(2,1)S(1)}, bf16[8,64,256]{2,1,0:T(8,128)(2,1)S(1)}, bf16[8,64,256]{2,1,0:T(8,128)(2,1)S(1)}, f32[8,8,128]{2,1,0:T(8,128)S(1)}, f32[8,4,8,256]{3,2,1,0:T(8,128)S(1)}) custom-call(bf16[8,160,2048]{2,1,0:T(8,128)(2,1)S(1)} %copy-done, bf16[8,64,256]{2,1,0:T(8,128)(2,1)S(1)} %bitcast.49, ...), custom_call_target="tpu_custom_call" | custom-call | tf_op jit(solution)/shard_map/give_back/pallas_call | solution.py:499
  197.6 0.7 convert_reduce_fusion
  198.3 7.3 %convolution_bitcast_fusion = f32[1,512,2048]{2,1,0:T(8,128)} fusion(bf16[8,160,512]{2,1,0:T(8,128)(2,1)S(1)} %copy-done.9, bf16[8,160,2048]{2,1,0:T(8,128)(2,1)} %get-tuple-element.32), kind=kOutput, calls=%fused_computation.5 | convolution fusion | flops 2684354560 | bytes 10747904 | tf_op jit(solution)/shard_map/dot_general | solution.py:611
  205.7 4.5 %convolution_bitcast_fusion.1 = f32[1,2048,512]{2,1,0:T(8,128)} fusion(bf16[8,160,2048]{2,1,0:T(8,128)(2,1)S(1)} %bitcast.67, bf16[8,160,512]{2,1,0:T(8,128)(2,1)S(1)} %copy-done.8), kind=kOutput, calls=%fused_computation.6 | convolution fusion | flops 2684354560 | bytes 10747904 | tf_op jit(solution)/shard_map/dot_general | solution.py:610
  210.1 4.4 %convolution_bitcast_fusion.2 = f32[1,2048,512]{2,1,0:T(8,128)} fusion(bf16[8,160,2048]{2,1,0:T(8,128)(2,1)S(1)} %bitcast.67, bf16[8,160,512]{2,1,0:T(8,128)(2,1)S(1)} %copy-done.7), kind=kOutput, calls=%fused_computation.7 | convolution fusion | flops 2684354560 | bytes 10747904 | tf_op jit(solution)/shard_map/dot_general | solution.py:609
  214.6 1.2 convolution_add_fusion.1
  215.9 1.5 fusion.3
  217.4 1.4 select_reduce_fusion
  (44 shorter events, 3.8 us)
Async XLA Ops:
  0.6 5.3 %copy-start.2 = (bf16[320,2048]{1,0:T(8,128)(2,1)S(1)}, bf16[320,2048]{1,0:T(8,128)(2,1)}, u32[]{:S(2)}) copy-start(bf16[320,2048]{1,0:T(8,128)(2,1)} %param.10) | copy-start | bytes 3932164
  6.0 2.3 %copy-start.3 = (bf16[320,2048]{1,0:T(8,128)(2,1)S(1)}, bf16[320,2048]{1,0:T(8,128)(2,1)}, u32[]{:S(2)}) copy-start(bf16[320,2048]{1,0:T(8,128)(2,1)} %param.11) | copy-start | bytes 3932164
  8.3 2.7 %copy-start.6 = (bf16[320,2]{0,1:T(2,128)(2,1)S(1)}, bf16[320,2]{0,1:T(2,128)(2,1)}, u32[]{:S(2)}) copy-start(bf16[320,2]{0,1:T(2,128)(2,1)} %param.13) | copy-start | bytes 3844
  130.3 1.8 copy-start.10
  132.1 0.7 copy-start.5
  136.9 2.7 %copy-start.4 = (bf16[320,2048]{1,0:T(8,128)(2,1)S(1)}, bf16[320,2048]{1,0:T(8,128)(2,1)}, u32[]{:S(2)}) copy-start(bf16[320,2048]{1,0:T(8,128)(2,1)} %fusion) | copy-start | bytes 3932164
  139.6 2.1 copy-start.1
  141.7 2.5 %copy-start = (bf16[8,160,2048]{2,1,0:T(8,128)(2,1)S(1)}, bf16[8,160,2048]{2,1,0:T(8,128)(2,1)}, u32[]{:S(2)}) copy-start(bf16[8,160,2048]{2,1,0:T(8,128)(2,1)} %get-tuple-element.24.part) | copy-start | bytes 15728644
  144.2 54.1 %copy-start.9 = (bf16[8,160,512]{2,1,0:T(8,128)(2,1)S(1)}, bf16[8,160,512]{2,1,0:T(8,128)(2,1)}, u32[]{:S(2)}) copy-start(bf16[8,160,512]{2,1,0:T(8,128)(2,1)} %get-tuple-element.31) | copy-start | bytes 3932164
  197.6 8.1 %slice-start = ((s8[5242880]{0:T(1024)(128)(4,1)}), s8[4194304]{0:T(1024)(128)(4,1)S(1)}, s32[]{:S(2)}) async-start(s8[5242880]{0:T(1024)(128)(4,1)} %bitcast.66), calls=%async_computation | async-start | bytes 8388608
  198.3 7.4 %slice-start.1 = ((s8[5242880]{0:T(1024)(128)(4,1)}), s8[1048576]{0:T(1024)(128)(4,1)S(1)}, s32[]{:S(2)}) async-start(s8[5242880]{0:T(1024)(128)(4,1)} %bitcast.66), calls=%async_computation.1 | async-start | bytes 2097152
  198.3 7.4 %copy-start.8 = (bf16[8,160,512]{2,1,0:T(8,128)(2,1)S(1)}, bf16[8,160,512]{2,1,0:T(8,128)(2,1)}, u32[]{:S(2)}) copy-start(bf16[8,160,512]{2,1,0:T(8,128)(2,1)} %get-tuple-element.30) | copy-start | bytes 3932164
  205.7 4.5 %copy-start.7 = (bf16[8,160,512]{2,1,0:T(8,128)(2,1)S(1)}, bf16[8,160,512]{2,1,0:T(8,128)(2,1)}, u32[]{:S(2)}) copy-start(bf16[8,160,512]{2,1,0:T(8,128)(2,1)} %get-tuple-element.29) | copy-start | bytes 3932164
where the time goes:
time: 220 us; the launch traced here: 219 us
  Pallas kernels  171 us (78%)
  matrix products  32 us (15%)
  other arithmetic  8.67 us (4%)
  local copies, waits for them, and re-layouts  6.67 us (3%)
    pallas_call x1, Pallas kernels, dispatch(): pl.pallas_call(functools.partial(dispatch_kernel, n_ep), out_shape=(rows,...  118 us
    pallas_call x1, Pallas kernels, give_back(): pl.pallas_call(functools.partial(return_kernel, n_ep, n_tp), out_shape=(j...  53.3 us
    dot_general x1, matrix products, shards(): lax.dot_general(act, scaled_cot, contract_rows, preferred_element_type=f32)  7.34 us
    dot_general x1, matrix products, shards(): lax.dot_general(x_slots, d_up, contract_rows, preferred_element_type=f32)  4.46 us
    dot_general x1, matrix products, shards(): lax.dot_general(x_slots, d_gate, contract_rows, preferred_element_type=f32)  4.44 us

commit v1 on v0

v1 whole, which is shorter than its diff:
```python
import functools
import types

import jax
import jax.numpy as jnp
from jax import lax
from jax.experimental import pallas as pl
from jax.experimental.pallas import tpu as pltpu
from jax.sharding import PartitionSpec as P

CLAMP_LIMIT = 7.0
SIG_SLOPE = 1.702
MESH = pl.DeviceIdType.MESH
ANY = pl.BlockSpec(memory_space=pl.ANY)
VMEM = pl.BlockSpec(memory_space=pltpu.VMEM)
CONTRACT_COLS = (((1,), (1,)), ((), ()))
CONTRACT_ROWS = (((0,), (0,)), ((), ()))
F32 = jnp.float32
BF = jnp.bfloat16


def layer_kernel(n_ep, n_tp, names, *refs):
    r = types.SimpleNamespace(**dict(zip(names, refs)))
    me = lax.axis_index("ep")
    t = lax.axis_index("tp")
    half = t // 2
    side = t % 2
    t_core = half * 2 + 1 - side
    t_x = (1 - half) * 2 + side
    cap, cols = r.x_send.shape[1:]
    tok_dev, width = r.tok.shape
    top_k = r.ids.shape[0]
    lanes = r.w_all.shape[2]
    core_peer = (me, t_core)
    x_peer = (me, t_x)
    log = n_ep.bit_length() - 1

    def dst(k):
        if 1 << log != n_ep:
            return lax.rem(me + k, n_ep)
        out = me
        for b in range(log):
            bit = (k // (1 << b)) % 2
            out = out + bit * (1 << b) * (1 - 2 * ((me // (1 << b)) % 2))
        return out

    def src(k):
        if 1 << log != n_ep:
            return lax.rem(me + n_ep - k, n_ep)
        return dst(k)

    def quarter(q):
        return pl.ds(pl.multiple_of(q * cols, cols), cols)

    def remote(source, target, sems, device):
        return pltpu.make_async_remote_copy(
            src_ref=source,
            dst_ref=target,
            send_sem=sems[0],
            recv_sem=sems[1],
            device_id=device,
            device_id_type=MESH,
        )

    loads = [
        pltpu.make_async_copy(a, b, r.load_sem.at[n])
        for n, (a, b) in enumerate(
            (
                (r.in_own, r.dense_all.at[me, t, 0]),
                (r.out_own, r.dense_all.at[me, t, 1]),
                (r.tokens, r.tok),
                (r.cotangent, r.cot),
                (r.w_gate, r.gate_w),
                (r.w_up, r.up_w),
                (r.w_down, r.down_w),
            )
        )
    ]
    for c in loads:
        c.start()

    peers = [(dst(k), t) for k in range(1, n_ep)] + [core_peer, x_peer]
    barrier = pltpu.get_barrier_semaphore()
    for device in peers:
        pl.semaphore_signal(barrier, inc=1, device_id=device, device_id_type=MESH)

    experts = r.pos.shape[0]
    expert_row = lax.broadcasted_iota(jnp.int32, (experts, tok_dev), 0)
    member = jnp.zeros((experts, tok_dev), F32)
    weight = jnp.zeros((experts, tok_dev), F32)
    for k in range(top_k):
        hit = r.ids[k : k + 1, :] == expert_row
        member = jnp.where(hit, 1.0, member)
        weight = jnp.where(hit, r.route[k : k + 1, :].astype(F32), weight)
    below = lax.broadcasted_iota(jnp.int32, (tok_dev, tok_dev), 0) < lax.broadcasted_iota(
        jnp.int32, (tok_dev, tok_dev), 1
    )
    rank = jnp.dot(
        member.astype(BF), jnp.where(below, 1.0, 0.0).astype(BF), preferred_element_type=F32
    )
    r.pos[...] = jnp.where(member > 0.0, rank, -1.0)
    r.weight[...] = weight
    r.w_send[...] = jnp.zeros(r.w_send.shape, F32)

    pl.semaphore_wait(barrier, len(peers))

    rows_send = (r.x_send, r.dy_send)
    rows_all = (r.x_all, r.dy_all)

    def shard_hop(kind, k):
        i = src(k)
        sems = (r.send_shard.at[kind, k], r.recv_shard.at[kind, k])
        if kind == 0:
            block = r.dense_all.at[me, t]
            return remote(block, block, sems, (dst(k), t))
        block = r.dense_all.at[i, t_x if kind == 3 else t]
        return remote(block, block, sems, x_peer if kind == 1 else core_peer)

    def row_hop(a, kind, k):
        i = src(k)
        sems = (r.send_rows.at[a, kind, k], r.recv_rows.at[a, kind, k])
        if kind == 0:
            return remote(
                rows_send[a].at[k], rows_all[a].at[me, :, quarter(t)], sems, (dst(k), t)
            )
        block = rows_all[a].at[i, :, quarter(t_x if kind == 3 else t)]
        return remote(block, block, sems, x_peer if kind == 1 else core_peer)

    def w_hop(k):
        return remote(
            r.w_send.at[k], r.w_all.at[me], (r.send_w.at[k], r.recv_w.at[k]), (dst(k), t)
        )

    loads[0].wait()
    loads[1].wait()
    shard_hop(1, 0).start()
    shard_hop(2, 0).start()

    @pl.loop(1, n_ep)
    def _(k):
        shard_hop(0, k).start()

    loads[2].wait()
    loads[3].wait()
    slot = lax.broadcasted_iota(jnp.int32, (cap, tok_dev), 0).astype(F32)

    def pick_rows(e):
        pick = jnp.where(slot == r.pos[pl.ds(e, 1), :], 1.0, 0.0).astype(BF)
        r.picks[e] = pick
        wide = jnp.broadcast_to(r.weight[pl.ds(e, 1), :], (16, tok_dev)).astype(BF)
        sent = lax.dot_general(wide, pick, CONTRACT_COLS, preferred_element_type=F32)
        return pick, sent[:8]

    @pl.loop(1, n_ep + 1)
    def _(k):
        @pl.when(k < n_ep)
        def _():
            pick, sent = pick_rows(dst(k))
            r.w_send[k, :, :cap] = sent
            r.x_send[k] = jnp.dot(
                pick, r.tok[:, quarter(t)], preferred_element_type=F32
            ).astype(BF)
            r.dy_send[k] = jnp.dot(
                pick, r.cot[:, quarter(t)], preferred_element_type=F32
            ).astype(BF)

        @pl.when(k > 1)
        def _():
            w_hop(k - 1).start()
            for a in range(2):
                row_hop(a, 0, k - 1).start()

    pick, sent = pick_rows(me)
    r.w_all[me] = jnp.zeros((8, lanes), F32)
    r.w_all[me, :, :cap] = sent

    @pl.loop(0, n_tp)
    def _(q):
        r.x_all[me, :, quarter(q)] = jnp.dot(
            pick, r.tok[:, quarter(q)], preferred_element_type=F32
        ).astype(BF)
        r.dy_all[me, :, quarter(q)] = jnp.dot(
            pick, r.cot[:, quarter(q)], preferred_element_type=F32
        ).astype(BF)

    for c in loads[4:]:
        c.wait()

    diagonal = lax.broadcasted_iota(jnp.int32, (cap, lanes), 0) == lax.broadcasted_iota(
        jnp.int32, (cap, lanes), 1
    )

    def compute(i):
        weight_row = r.w_all[i, 0:1]
        route_col = jnp.sum(jnp.where(diagonal, weight_row, 0.0), axis=1, keepdims=True)
        x_rows = r.x_all[i]
        gate_pre = jnp.dot(x_rows, r.gate_w[...], preferred_element_type=F32)
        up_pre = jnp.dot(x_rows, r.up_w[...], preferred_element_type=F32)
        gate_clamp = jnp.minimum(gate_pre, CLAMP_LIMIT)
        up_clamp = jnp.clip(up_pre, -CLAMP_LIMIT, CLAMP_LIMIT)
        sig = jax.nn.sigmoid(SIG_SLOPE * gate_clamp)
        act = (gate_clamp * sig * (up_clamp + 1.0)).astype(BF)
        r.act[i] = act
        dy_rows = r.dy_all[i]
        r.scaled[i] = (route_col * dy_rows.astype(F32)).astype(BF)
        back = lax.dot_general(dy_rows, r.down_w[...], CONTRACT_COLS, preferred_element_type=F32)
        weight_sum = jnp.sum(act.astype(F32) * back, axis=1, keepdims=True)
        r.w_part[pl.ds(i, 1), :] = jnp.sum(
            jnp.where(diagonal, weight_sum, 0.0), axis=0, keepdims=True
        )
        d_act = route_col * back
        d_gate = jnp.where(
            gate_pre < CLAMP_LIMIT,
            d_act * (up_clamp + 1.0) * (sig + SIG_SLOPE * gate_clamp * sig * (1.0 - sig)),
            0.0,
        ).astype(BF)
        d_up = jnp.where(jnp.abs(up_pre) < CLAMP_LIMIT, d_act * gate_clamp * sig, 0.0).astype(BF)
        r.d_gate[i] = d_gate
        r.d_up[i] = d_up
        part = lax.dot_general(d_gate, r.gate_w[...], CONTRACT_COLS, preferred_element_type=F32)
        part = part + lax.dot_general(
            d_up, r.up_w[...], CONTRACT_COLS, preferred_element_type=F32
        )
        r.part[i] = part.astype(BF)

    def back_core(k, h):
        return remote(
            r.part.at[src(k), :, quarter(h * 2 + 1 - side)],
            r.from_core.at[k, h],
            (r.send_bc.at[k, h], r.recv_bc.at[k, h]),
            core_peer,
        )

    def back_x(k):
        return remote(r.to_x.at[k], r.from_x.at[k], (r.send_bx.at[k], r.recv_bx.at[k]), x_peer)

    def back_ep(k):
        return remote(
            r.to_ep.at[k],
            r.rows_back.at[me],
            (r.send_be.at[k], r.recv_be.at[k]),
            (src(k), t),
        )

    def run(k):
        compute(src(k))
        for h in range(2):
            back_core(k, h).start()

    def sum_core(k):
        for h in range(2):
            back_core(k, h).wait_recv()
        other = r.part[src(k), :, quarter(t_x)].astype(F32)
        r.to_x[k] = (other + r.from_core[k, 1 - half].astype(F32)).astype(BF)
        back_x(k).start()

    def sum_x(k):
        back_x(k).wait_recv()
        mine = r.part[src(k), :, quarter(t)].astype(F32)
        mine = mine + r.from_core[k, half].astype(F32)
        return (mine + r.from_x[k].astype(F32)).astype(BF)

    def send_back(k):
        r.to_ep[k] = sum_x(k)
        back_ep(k).start()

    def grad_hop(k):
        return remote(
            r.dg_send.at[dst(k)], r.dg_back.at[me], (r.send_dg.at[k], r.recv_dg.at[k]), (dst(k), t)
        )

    def gate_hop(k):
        return remote(
            r.gg_send.at[dst(k)], r.gg_back.at[me], (r.send_gg.at[k], r.recv_gg.at[k]), (dst(k), t)
        )

    own_rows, rank_r = r.in_own.shape
    span = n_ep // n_tp
    block_cols = width // n_ep

    def dense():
        in_whole = r.dense_all[:, :, 0].reshape(width, rank_r)
        out_whole = r.dense_all[:, :, 1].reshape(width, rank_r)
        pre = jnp.dot(r.tok[...], in_whole, preferred_element_type=F32)
        cob = jnp.dot(r.cot[...], out_whole, preferred_element_type=F32)
        gate_wide = jnp.broadcast_to(r.gate_row[...].astype(F32), (16, width)).astype(BF)
        logit = lax.dot_general(
            r.tok[...], gate_wide, CONTRACT_COLS, preferred_element_type=F32
        )[:, :1]
        mix = jax.nn.sigmoid(logit)
        sig = jax.nn.sigmoid(pre)
        act = (pre * sig).astype(BF)
        dpre = (mix * cob * sig * (1.0 + pre * (1.0 - sig))).astype(BF)
        act_wide = act.astype(F32)
        dlogit = mix * (1.0 - mix) * jnp.sum(act_wide * cob, axis=1, keepdims=True)
        in_rows = r.dense_all[pl.ds(t * span, span), :, 0].reshape(cols, rank_r)
        dx = lax.dot_general(dpre, in_rows, CONTRACT_COLS, preferred_element_type=F32)
        r.dense_dx[...] = dx + dlogit * r.gate_row[:, quarter(t)].astype(F32)
        lane = lax.broadcasted_iota(jnp.int32, (tok_dev, 128), 1)
        high = dlogit.astype(BF).astype(F32)
        low = dlogit - high
        pair = jnp.where(lane == 0, high, jnp.where(lane == 1, low, 0.0)).astype(BF)
        gate_sum = lax.dot_general(pair, r.tok[...], CONTRACT_ROWS, preferred_element_type=F32)
        gate_sum = gate_sum[0:1] + gate_sum[1:2]
        for e in range(n_ep):
            r.gg_send[e, :, :block_cols] = jnp.broadcast_to(
                gate_sum[:, e * block_cols : (e + 1) * block_cols], (8, block_cols)
            )
        mixed = (mix * act_wide).astype(BF)
        for a, (left, right) in enumerate(((r.tok, dpre), (r.cot, mixed))):
            r.dense_grad[...] = lax.dot_general(
                left[...], right, CONTRACT_ROWS, preferred_element_type=F32
            )
            for e in range(n_ep):
                start = pl.multiple_of((e * n_tp + t) * own_rows, own_rows)
                r.dg_send[e, a] = r.dense_grad[pl.ds(start, own_rows), :].astype(BF)
        r.dg_back[me] = r.dg_send[me]
        r.gg_back[me] = r.gg_send[me]

        @pl.loop(1, n_ep)
        def _(k):
            gate_hop(k).start()
            grad_hop(k).start()

    shard_steps = (n_ep - 1 + 1) // 2

    @pl.loop(0, n_ep + 2)
    def _(n):
        for b in (2 * n - 1, 2 * n):

            @pl.when((b >= 1) & (b < n_ep))
            def _():
                shard_hop(0, b).wait_recv()
                shard_hop(1, b).start()
                shard_hop(2, b).start()

        @pl.when((n >= 1) & (n < n_ep))
        def _():
            for a in range(2):
                row_hop(a, 0, n).wait_recv()
                row_hop(a, 1, n).start()
                row_hop(a, 2, n).start()
            w_hop(n).wait_recv()

        @pl.when(n >= 3)
        def _():
            sum_core(n - 3)

        @pl.when(n == 4)
        def _():
            r.rows_back[me] = sum_x(0)

        @pl.when(n >= 5)
        def _():
            send_back(n - 4)

        @pl.when((n == 0) | (n >= 3))
        def _():
            k = jnp.where(n == 0, 0, n - 2)

            @pl.when(n >= 3)
            def _():
                for a in range(2):
                    for kind in (2, 3):
                        row_hop(a, kind, k).wait_recv()

            run(k)

        for b in (2 * n - 3, 2 * n - 2):

            @pl.when((b >= 0) & (b < n_ep))
            def _():
                shard_hop(1, b).wait_recv()
                shard_hop(3, b).start()

        @pl.when((n >= 2) & (n < n_ep + 1))
        def _():
            for a in range(2):
                row_hop(a, 1, n - 1).wait_recv()
                row_hop(a, 3, n - 1).start()

        @pl.when(n == shard_steps + 2)
        def _():
            @pl.loop(0, n_ep)
            def _(k):
                for kind in (2, 3):
                    shard_hop(kind, k).wait_recv()

            dense()

    rows = n_ep * cap
    stages = r.stage.shape[0]
    tiles = width // cols

    def tile_out(kind, j, slot_index):
        number = kind * tiles + j
        target = (
            r.grad_down.at[:, quarter(j)]
            if kind == 0
            else (r.grad_gate if kind == 1 else r.grad_up).at[quarter(j), :]
        )
        return pltpu.make_async_copy(
            r.stage.at[slot_index, : target.shape[0], : target.shape[1]],
            target,
            r.tile_sem.at[number],
        )

    def tile(kind, j):
        number = kind * tiles + j
        s = number % stages
        if number >= stages:
            old = number - stages
            tile_out(old // tiles, old % tiles, s).wait()
        if kind == 0:
            left = r.act[...].reshape(rows, -1)
            right = r.scaled.reshape(rows, width)[:, quarter(j)]
        else:
            left = r.x_all.reshape(rows, width)[:, quarter(j)]
            right = (r.d_gate if kind == 1 else r.d_up)[...].reshape(rows, -1)
        r.stage[s] = lax.dot_general(left, right, CONTRACT_ROWS, preferred_element_type=F32)
        tile_out(kind, j, s).start()

    def weight_core():
        return remote(r.w_part, r.w_from.at[0], (r.send_wt.at[0], r.recv_wt.at[0]), core_peer)

    def weight_x():
        return remote(r.w_half, r.w_from.at[1], (r.send_wt.at[1], r.recv_wt.at[1]), x_peer)

    def weight_ep(k):
        return remote(
            r.w_sum, r.w_back.at[me], (r.send_we.at[k], r.recv_we.at[k]), (src(k), t)
        )

    weight_core().start()
    tile(0, 0)
    sum_core(n_ep - 1)
    weight_core().wait_recv()
    r.w_half[...] = r.w_part[...] + r.w_from[0]
    send_back(n_ep - 2)
    weight_x().start()
    for j in range(1, tiles):
        tile(0, j)
    weight_x().wait_recv()
    r.w_sum[...] = r.w_half[...] + r.w_from[1]
    send_back(n_ep - 1)
    r.w_back[me] = r.w_sum[...]

    @pl.loop(1, n_ep)
    def _(k):
        weight_ep(k).start()

    for kind in (1, 2):
        for j in range(tiles):
            tile(kind, j)

    @pl.loop(1, n_ep)
    def _(k):
        grad_hop(k).wait_recv()
        gate_hop(k).wait_recv()

    total = jnp.zeros((2, own_rows, rank_r), F32)
    gate_total = jnp.zeros(r.gg_out.shape, F32)
    for e in range(n_ep):
        total = total + r.dg_back[e].astype(F32)
        gate_total = gate_total + r.gg_back[e]
    r.dg_out[...] = total
    r.gg_out[...] = gate_total

    @pl.loop(1, n_ep)
    def _(k):
        weight_ep(k).wait_recv()
        back_ep(k).wait_recv()

    picks = r.picks[...].reshape(rows, tok_dev)
    moved = lax.dot_general(
        picks,
        r.rows_back[...].reshape(rows, cols),
        CONTRACT_ROWS,
        preferred_element_type=F32,
    )
    r.grad_tokens[...] = (r.dense_dx[...] + moved).astype(BF)
    found = [jnp.zeros((1, tok_dev), F32) for _ in range(top_k)]
    for e in range(n_ep):
        row = r.w_back[e, pl.ds(me, 1), :]
        row = jnp.broadcast_to(row, (16, lanes)).astype(BF)[:, :cap]
        spread = jnp.dot(row, r.picks[e], preferred_element_type=F32)[0:1]
        for k in range(top_k):
            found[k] = found[k] + jnp.where(r.ids[k : k + 1, :] == e, spread, 0.0)
    for k in range(top_k):
        r.grad_route[k : k + 1, :] = found[k].astype(BF)

    @pl.loop(0, n_ep)
    def _(k):
        for kind in (1, 2, 3):
            shard_hop(kind, k).wait_send()
        for h in range(2):
            back_core(k, h).wait_send()
        back_x(k).wait_send()

    @pl.loop(1, n_ep)
    def _(k):
        shard_hop(0, k).wait_send()
        for a in range(2):
            for kind in range(4):
                row_hop(a, kind, k).wait_send()
        w_hop(k).wait_send()
        back_ep(k).wait_send()
        weight_ep(k).wait_send()
        grad_hop(k).wait_send()
        gate_hop(k).wait_send()

    weight_core().wait_send()
    weight_x().wait_send()
    for number in range(3 * tiles - stages, 3 * tiles):
        tile_out(number // tiles, number % tiles, number % stages).wait()


def shards(
    tokens,
    cotangent,
    route_ids,
    route_weights,
    w_gate,
    w_up,
    w_down,
    dense_in,
    dense_out,
    dense_gate,
):
    n_ep = lax.axis_size("ep")
    n_tp = lax.axis_size("tp")
    tok_dev, width = tokens.shape
    top_k = route_ids.shape[1]
    cols = width // n_tp
    cap = 2 * tok_dev * top_k // n_ep
    lanes = -(-cap // 128) * 128
    hidden = w_gate.shape[2]
    own_rows, rank_r = dense_in.shape
    gate_lanes = -(-(width // n_ep) // 128) * 128
    dma = pltpu.SemaphoreType.DMA
    stages = 3
    args = dict(
        ids=(route_ids.T, VMEM),
        route=(route_weights.T, VMEM),
        gate_row=(dense_gate[None], VMEM),
        tokens=(tokens, ANY),
        cotangent=(cotangent, ANY),
        in_own=(dense_in, ANY),
        out_own=(dense_out, ANY),
        w_gate=(w_gate[0], ANY),
        w_up=(w_up[0], ANY),
        w_down=(w_down[0], ANY),
    )
    outs = dict(
        grad_tokens=((tok_dev, cols), BF, VMEM),
        grad_route=((top_k, tok_dev), BF, VMEM),
        grad_gate=((width, hidden), F32, ANY),
        grad_up=((width, hidden), F32, ANY),
        grad_down=((hidden, width), F32, ANY),
        dg_out=((2, own_rows, rank_r), F32, VMEM),
        gg_out=((8, gate_lanes), F32, VMEM),
    )
    scratch = dict(
        tok=((tok_dev, width), BF),
        cot=((tok_dev, width), BF),
        gate_w=((width, hidden), BF),
        up_w=((width, hidden), BF),
        down_w=((hidden, width), BF),
        pos=((max(16, n_ep), tok_dev), F32),
        weight=((max(16, n_ep), tok_dev), F32),
        picks=((n_ep, cap, tok_dev), BF),
        w_send=((n_ep, 8, lanes), F32),
        w_all=((n_ep, 8, lanes), F32),
        x_send=((n_ep, cap, cols), BF),
        dy_send=((n_ep, cap, cols), BF),
        x_all=((n_ep, cap, width), BF),
        dy_all=((n_ep, cap, width), BF),
        scaled=((n_ep, cap, width), BF),
        act=((n_ep, cap, hidden), BF),
        d_gate=((n_ep, cap, hidden), BF),
        d_up=((n_ep, cap, hidden), BF),
        part=((n_ep, cap, width), BF),
        w_part=((n_ep, lanes), F32),
        from_core=((n_ep, 2, cap, cols), BF),
        to_x=((n_ep, cap, cols), BF),
        from_x=((n_ep, cap, cols), BF),
        to_ep=((n_ep, cap, cols), BF),
        rows_back=((n_ep, cap, cols), BF),
        dense_all=((n_ep, n_tp, 2, own_rows, rank_r), BF),
        dense_dx=((tok_dev, cols), F32),
        dense_grad=((width, rank_r), F32),
        dg_send=((n_ep, 2, own_rows, rank_r), BF),
        dg_back=((n_ep, 2, own_rows, rank_r), BF),
        gg_send=((n_ep, 8, gate_lanes), F32),
        gg_back=((n_ep, 8, gate_lanes), F32),
        w_from=((2, n_ep, lanes), F32),
        w_half=((n_ep, lanes), F32),
        w_sum=((n_ep, lanes), F32),
        w_back=((n_ep, n_ep, lanes), F32),
        stage=((stages, cols, hidden), F32),
    )
    sems = dict(
        load_sem=(7,),
        send_rows=(2, 4, n_ep),
        recv_rows=(2, 4, n_ep),
        send_shard=(4, n_ep),
        recv_shard=(4, n_ep),
        send_w=(n_ep,),
        recv_w=(n_ep,),
        send_bc=(n_ep, 2),
        recv_bc=(n_ep, 2),
        send_bx=(n_ep,),
        recv_bx=(n_ep,),
        send_be=(n_ep,),
        recv_be=(n_ep,),
        send_dg=(n_ep,),
        recv_dg=(n_ep,),
        send_gg=(n_ep,),
        recv_gg=(n_ep,),
        send_wt=(2,),
        recv_wt=(2,),
        send_we=(n_ep,),
        recv_we=(n_ep,),
        tile_sem=(3 * (width // cols),),
    )
    names = list(args) + list(outs) + list(scratch) + list(sems)
    results = pl.pallas_call(
        functools.partial(layer_kernel, n_ep, n_tp, names),
        out_shape=tuple(jax.ShapeDtypeStruct(s, d) for s, d, _ in outs.values()),
        in_specs=[spec for _, spec in args.values()],
        out_specs=tuple(spec for _, _, spec in outs.values()),
        scratch_shapes=[pltpu.VMEM(s, d) for s, d in scratch.values()]
        + [dma(s) for s in sems.values()],
        compiler_params=pltpu.CompilerParams(
            collective_id=0, has_side_effects=True, vmem_limit_bytes=63 * 1024 * 1024
        ),
        name="layer",
    )(*(a for a, _ in args.values()))
    grad_tokens, grad_route, grad_gate, grad_up, grad_down, dg_out, gg_out = results
    block = width // (n_ep * n_tp)
    grad_dense_gate = lax.dynamic_slice_in_dim(gg_out[0], lax.axis_index("tp") * block, block)
    return (
        grad_tokens,
        grad_route.T,
        grad_gate[None],
        grad_up[None],
        grad_down[None],
        dg_out[0],
        dg_out[1],
        grad_dense_gate,
    )


def solution(mesh):
    placed = (
        P("ep", None),
        P("ep", None),
        P("ep", None),
        P("ep", None),
        P("ep", None, "tp"),
        P("ep", None, "tp"),
        P("ep", "tp", None),
        P(("ep", "tp"), None),
        P(("ep", "tp"), None),
        P(),
    )
    return jax.shard_map(
        shards,
        mesh=mesh,
        in_specs=placed,
        out_specs=(
            P("ep", "tp"),
            P("ep", None),
            P("ep", None, "tp"),
            P("ep", None, "tp"),
            P("ep", "tp", None),
            P(("ep", "tp"), None),
            P(("ep", "tp"), None),
            P(("ep", "tp")),
        ),
        check_vma=False,
    )
```

time: 220 us -> 149 us (0.68)
  the two profiles are of different devices: /device:TPU:12 before, /device:TPU:0 now
where the time goes in v1:
time: 149 us
  Pallas kernels  130 us (87%)
  local copies, waits for them, and re-layouts  17.6 us (12%)
    pallas_call x1, Pallas kernels, shards(): pl.pallas_call(functools.partial(layer_kernel, n_ep, n_tp, names), out_sh...  130 us
    unnamed x9, local copies, waits for them, and re-layouts  13.5 us

profile of v1, /device:TPU:0, one launch (start us, length us, event | category | flops | bytes accessed | tf_op | source)
XLA Modules:
  0.0 148.7 jit_solution(8100720677072796801)
XLA Ops:
  0.6 1.3 broadcast_in_dim.12.refs_2_
  1.9 130.4 %layer.1 = (bf16[320,512]{1,0:T(8,128)(2,1)}, bf16[2,320]{1,0:T(2,128)(2,1)}, f32[2048,512]{1,0:T(8,128)}, f32[2048,512]{1,0:T(8,128)}, f32[512,2048]{1,0:T(8,12...) custom-call(s32[2,320]{1,0:T(2,128)} %bitcast.21, bf16[2,320]{1,0:T(2,128)(2,1)} %bitcast.22, ...), custom_call_target="tpu_custom_call" | custom-call | tf_op jit(solution)/shard_map/layer/pallas_call | solution.py:627
  132.4 0.7 slice.11
  133.1 0.6 dynamic-slice_bitcast_fusion
  133.6 1.5 %slice_bitcast_fusion = (f32[64,256]{1,0:T(8,128)}, f32[64,256]{1,0:T(8,128)}) fusion(f32[2,64,256]{2,1,0:T(8,128)} %get-tuple-element.20), kind=kLoop, calls=%fused_computation | loop fusion | bytes 262144 | tf_op jit(solution)/shard_map/squeeze | solution.py:649
  135.2 1.7 %copy.23 = bf16[320,512]{1,0:T(8,128)(2,1)} copy(bf16[320,512]{1,0:T(8,128)(2,1)} %get-tuple-element.32) | data formatting | bytes 655360
  136.9 1.2 copy.24
  138.1 0.0 copy-start.1
  138.1 4.8 %copy.25 = f32[1,2048,512]{2,1,0:T(8,128)} copy(f32[1,2048,512]{2,1,0:T(8,128)} %bitcast.17) | data formatting | bytes 8388608
  143.0 0.0 copy-done.1
  143.0 0.0 copy-start
  143.0 2.1 %copy.26 = f32[1,2048,512]{2,1,0:T(8,128)} copy(f32[1,2048,512]{2,1,0:T(8,128)S(1)} %bitcast.16) | data formatting | bytes 8388608
  145.1 1.6 %copy-done = f32[512,2048]{1,0:T(8,128)S(1)} copy-done((f32[512,2048]{1,0:T(8,128)S(1)}, f32[512,2048]{1,0:T(8,128)}, u32[]{:S(2)}) %copy-start) | copy-done | bytes 4194328
  146.7 2.0 %copy.27 = f32[1,512,2048]{2,1,0:T(8,128)} copy(f32[1,512,2048]{2,1,0:T(8,128)S(1)} %bitcast.15) | data formatting | bytes 8388608
Async XLA Ops:
  138.1 4.8 %copy-start.1 = (f32[2048,512]{1,0:T(8,128)S(1)}, f32[2048,512]{1,0:T(8,128)}, u32[]{:S(2)}) copy-start(f32[2048,512]{1,0:T(8,128)} %get-tuple-element.18) | copy-start | bytes 12582916
  143.0 3.7 %copy-start = (f32[512,2048]{1,0:T(8,128)S(1)}, f32[512,2048]{1,0:T(8,128)}, u32[]{:S(2)}) copy-start(f32[512,2048]{1,0:T(8,128)} %get-tuple-element.19) | copy-start | bytes 12582916

commit v2 on v1

v2 whole, which is shorter than its diff:
```python
import functools
import types

import jax
import jax.numpy as jnp
from jax import lax
from jax.experimental import pallas as pl
from jax.experimental.pallas import tpu as pltpu
from jax.sharding import PartitionSpec as P

CLAMP_LIMIT = 7.0
SIG_SLOPE = 1.702
MESH = pl.DeviceIdType.MESH
ANY = pl.BlockSpec(memory_space=pl.ANY)
VMEM = pl.BlockSpec(memory_space=pltpu.VMEM)
CONTRACT_COLS = (((1,), (1,)), ((), ()))
CONTRACT_ROWS = (((0,), (0,)), ((), ()))
F32 = jnp.float32
BF = jnp.bfloat16


def layer_kernel(n_ep, n_tp, names, *refs):
    r = types.SimpleNamespace(**dict(zip(names, refs)))
    me = lax.axis_index("ep")
    t = lax.axis_index("tp")
    half = t // 2
    side = t % 2
    t_core = half * 2 + 1 - side
    t_x = (1 - half) * 2 + side
    cap, cols = r.x_send.shape[1:]
    tok_dev, width = r.tok.shape
    top_k = r.ids.shape[0]
    lanes = r.w_all.shape[2]
    core_peer = (me, t_core)
    x_peer = (me, t_x)
    log = n_ep.bit_length() - 1
    near = n_ep // 4

    def dst(k):
        out = me
        for b in range(log):
            bit = (k // (1 << b)) % 2
            out = out + bit * (1 << b) * (1 - 2 * ((me // (1 << b)) % 2))
        return out

    src = dst
    planes = n_ep // near
    z = me // near
    inner = ((z + 1) // 2) % 2

    def seq(n):
        p = n + near - 1
        f = p // near
        k = jnp.where((f >= 2) & (inner == 1), (5 - f) * near + p % near, p)
        k = jnp.where(n > n_ep - near, n - (n_ep - near), k)
        return jnp.where(n == 0, 0, k)

    def quarter(q):
        return pl.ds(pl.multiple_of(q * cols, cols), cols)

    def remote(source, target, sems, device):
        return pltpu.make_async_remote_copy(
            src_ref=source,
            dst_ref=target,
            send_sem=sems[0],
            recv_sem=sems[1],
            device_id=device,
            device_id_type=MESH,
        )

    loads = [
        pltpu.make_async_copy(a, b, r.load_sem.at[n])
        for n, (a, b) in enumerate(
            (
                (r.in_own, r.dense_all.at[me, t, 0]),
                (r.out_own, r.dense_all.at[me, t, 1]),
                (r.tokens, r.tok),
                (r.cotangent, r.cot),
                (r.w_gate, r.gate_w),
                (r.w_up, r.up_w),
                (r.w_down, r.down_w),
            )
        )
    ]
    for c in loads:
        c.start()

    r.w_all[...] = jnp.zeros(r.w_all.shape, F32)
    peers = [(dst(k), t) for k in range(1, n_ep)] + [core_peer, x_peer]
    barrier = pltpu.get_barrier_semaphore()
    for device in peers:
        pl.semaphore_signal(barrier, inc=1, device_id=device, device_id_type=MESH)

    experts = r.pos.shape[0]
    expert_row = lax.broadcasted_iota(jnp.int32, (experts, tok_dev), 0)
    below = lax.broadcasted_iota(jnp.int32, (tok_dev, tok_dev), 0) < lax.broadcasted_iota(
        jnp.int32, (tok_dev, tok_dev), 1
    )
    r.below[...] = jnp.where(below, 1.0, 0.0).astype(BF)

    def place(s, pos, weight):
        member = jnp.zeros((experts, tok_dev), F32)
        scale = jnp.zeros((experts, tok_dev), F32)
        for k in range(top_k):
            hit = r.ids_all[s, k : k + 1, :] == expert_row
            member = jnp.where(hit, 1.0, member)
            scale = jnp.where(hit, r.route_all[s, k : k + 1, :], scale)
        rank = jnp.dot(member.astype(BF), r.below[...], preferred_element_type=F32)
        pos[...] = jnp.where(member > 0.0, rank, -1.0)
        weight[...] = scale

    r.ids_all[z] = r.ids[...]
    r.route_all[z] = r.route[...].astype(F32)
    place(z, r.own_pos, r.own_weight)
    r.w_send[...] = jnp.zeros(r.w_send.shape, F32)

    pl.semaphore_wait(barrier, len(peers))

    rows_send = (r.x_send, r.dy_send)
    extra_send = (r.x_extra, r.dy_extra)
    rows_all = (r.x_all, r.dy_all)

    def shard_hop(kind, k):
        sems = (r.send_shard.at[kind, k], r.recv_shard.at[kind, k])
        if kind == 0:
            block = r.dense_all.at[me, t]
            return remote(block, block, sems, (dst(k), t))
        if kind >= 4:
            block = r.dense_all.at[dst(k - k % near), t if kind == 4 else t_x]
            return remote(block, block, sems, (dst(k % near), t))
        block = r.dense_all.at[src(k), t_x if kind == 3 else t]
        return remote(block, block, sems, x_peer if kind == 1 else core_peer)

    def row_hop(a, kind, k):
        i = src(k)
        sems = (r.send_rows.at[a, kind, k], r.recv_rows.at[a, kind, k])
        if kind == 0:
            c = k % near
            return remote(
                rows_send[a].at[k], rows_all[a].at[dst(k - c), :, quarter(t)], sems, (dst(c), t)
            )
        if kind == 4:
            return remote(
                extra_send[a].at[k],
                rows_all[a].at[me, :, quarter(t_x)],
                (r.send_rows.at[a, 1, k], r.recv_rows.at[a, 1, k]),
                (dst(k), t),
            )
        block = rows_all[a].at[i, :, quarter(t_x if kind == 3 else t)]
        return remote(block, block, sems, x_peer if kind == 1 else core_peer)

    def w_hop(k):
        c = k % near
        return remote(
            r.w_send.at[k],
            r.w_all.at[dst(k - c)],
            (r.send_w.at[k], r.recv_w.at[k]),
            (dst(c), t),
        )

    own_raw = (r.tok, r.cot)
    raw = (r.x_raw, r.dy_raw)

    def raw_hop(a, s, up, own=False):
        plane = z + 1 if up else z - 1
        source = own_raw[a].at[:, quarter(t)] if own else raw[a].at[s]
        return remote(
            source,
            raw[a].at[s],
            (r.send_raw.at[a, int(up), s], r.recv_raw.at[a, s]),
            (plane * near + me % near, t),
        )

    def each_raw(a, s, act):
        @pl.when((s < z) & (z < planes - 1))
        def _():
            act(raw_hop(a, s, True))

        @pl.when((s > z) & (z > 0))
        def _():
            act(raw_hop(a, s, False))

    def each_own(a, act):
        @pl.when(z < planes - 1)
        def _():
            act(raw_hop(a, z, True, True))

        @pl.when(z > 0)
        def _():
            act(raw_hop(a, z, False, True))

    def pass_on(a, f):
        s = dst(f * near) // near
        raw_hop(a, s, False).wait_recv()
        each_raw(a, s, lambda copy: copy.start())

    def info_hop(kind, f):
        array = (r.ids_all, r.route_all)[kind]
        return remote(
            array.at[z],
            array.at[z],
            (r.send_info.at[kind, f], r.recv_info.at[kind, f]),
            (dst(f * near), t),
        )

    for f in range(1, planes):
        for kind in range(2):
            info_hop(kind, f).start()
    loads[2].wait()
    each_own(0, lambda c: c.start())
    loads[3].wait()
    each_own(1, lambda c: c.start())
    loads[0].wait()
    loads[1].wait()
    shard_hop(1, 0).start()
    shard_hop(2, 0).start()

    for k in range(near, n_ep, near):
        shard_hop(0, k).start()
    for k in range(1, near):
        shard_hop(4, k).start()

    slot = lax.broadcasted_iota(jnp.int32, (cap, tok_dev), 0).astype(F32)

    def pick_of(pos, e):
        return jnp.where(slot == pos[pl.ds(e, 1), :], 1.0, 0.0).astype(BF)

    def pick_rows(pos, weight, e):
        pick = pick_of(pos, e)
        wide = jnp.broadcast_to(weight[pl.ds(e, 1), :], (16, tok_dev)).astype(BF)
        sent = lax.dot_general(wide, pick, CONTRACT_COLS, preferred_element_type=F32)
        return pick, sent[:1]

    def picked(pick, rows):
        return jnp.dot(pick, rows, preferred_element_type=F32).astype(BF)

    def pick_close(a, k, pos, rows):
        @pl.loop(1, near)
        def _(c):
            rows_send[a][k + c] = picked(pick_of(pos, dst(c)), rows())

    def send_close(a, k):
        @pl.loop(1, near)
        def _(c):
            row_hop(a, 0, k + c).start()

    def weigh_close(k, pos, weight):
        @pl.loop(1, near)
        def _(c):
            _, sent = pick_rows(pos, weight, dst(c))
            r.w_send[k + c, :, :cap] = sent
            w_hop(k + c).start()

    for a in range(2):
        pick_close(a, 0, r.own_pos, lambda: own_raw[a][:, quarter(t)])
    for a in range(2):
        send_close(a, 0)
    pick, sent = pick_rows(r.own_pos, r.own_weight, me)
    r.w_all[me, :, :cap] = sent
    weigh_close(0, r.own_pos, r.own_weight)

    @pl.loop(1, near)
    def _(c):
        extra, _ = pick_rows(r.own_pos, r.own_weight, dst(c))
        r.x_extra[c] = picked(extra, r.tok[:, quarter(t_x)])
        r.dy_extra[c] = picked(extra, r.cot[:, quarter(t_x)])

    @pl.loop(0, n_tp)
    def _(q):
        r.x_all[me, :, quarter(q)] = jnp.dot(
            pick, r.tok[:, quarter(q)], preferred_element_type=F32
        ).astype(BF)
        r.dy_all[me, :, quarter(q)] = jnp.dot(
            pick, r.cot[:, quarter(q)], preferred_element_type=F32
        ).astype(BF)

    @pl.loop(1, near)
    def _(c):
        for a in range(2):
            row_hop(a, 4, c).start()

    for c in loads[4:]:
        c.wait()

    diagonal = lax.broadcasted_iota(jnp.int32, (cap, lanes), 0) == lax.broadcasted_iota(
        jnp.int32, (cap, lanes), 1
    )

    def compute(i):
        weight_row = r.w_all[i]
        route_col = jnp.sum(jnp.where(diagonal, weight_row, 0.0), axis=1, keepdims=True)
        x_rows = r.x_all[i]
        gate_pre = jnp.dot(x_rows, r.gate_w[...], preferred_element_type=F32)
        up_pre = jnp.dot(x_rows, r.up_w[...], preferred_element_type=F32)
        gate_clamp = jnp.minimum(gate_pre, CLAMP_LIMIT)
        up_clamp = jnp.clip(up_pre, -CLAMP_LIMIT, CLAMP_LIMIT)
        sig = jax.nn.sigmoid(SIG_SLOPE * gate_clamp)
        act = (gate_clamp * sig * (up_clamp + 1.0)).astype(BF)
        act_wide = act.astype(F32)
        r.act[i] = (route_col * act_wide).astype(BF)
        dy_rows = r.dy_all[i]
        back = lax.dot_general(dy_rows, r.down_w[...], CONTRACT_COLS, preferred_element_type=F32)
        weight_sum = jnp.sum(act_wide * back, axis=1, keepdims=True)
        r.w_part[i] = jnp.sum(
            jnp.where(diagonal, weight_sum, 0.0), axis=0, keepdims=True
        )
        d_act = route_col * back
        d_gate = jnp.where(
            gate_pre < CLAMP_LIMIT,
            d_act * (up_clamp + 1.0) * (sig + SIG_SLOPE * gate_clamp * sig * (1.0 - sig)),
            0.0,
        ).astype(BF)
        d_up = jnp.where(jnp.abs(up_pre) < CLAMP_LIMIT, d_act * gate_clamp * sig, 0.0).astype(BF)
        r.d_gate[i] = d_gate
        r.d_up[i] = d_up
        part = lax.dot_general(d_gate, r.gate_w[...], CONTRACT_COLS, preferred_element_type=F32)
        part = part + lax.dot_general(
            d_up, r.up_w[...], CONTRACT_COLS, preferred_element_type=F32
        )
        r.part[i] = part.astype(BF)

    def back_core(k, h):
        return remote(
            r.part.at[src(k), :, quarter(h * 2 + 1 - side)],
            r.from_core.at[k, h],
            (r.send_bc.at[k, h], r.recv_bc.at[k, h]),
            core_peer,
        )

    def back_x(k):
        return remote(
            r.part.at[src(k), :, quarter(t_x)],
            r.from_x.at[k],
            (r.send_bx.at[k], r.recv_bx.at[k]),
            x_peer,
        )

    def back_ep(k):
        return remote(
            r.part.at[src(k), :, quarter(t)],
            r.rows_back.at[me],
            (r.send_be.at[k], r.recv_be.at[k]),
            (src(k), t),
        )

    def run(k):
        compute(src(k))
        for h in range(2):
            back_core(k, h).start()

    def sum_core(k):
        for h in range(2):
            back_core(k, h).wait_recv()
        other = r.part[src(k), :, quarter(t_x)].astype(F32)
        other = other + r.from_core[k, 1 - half].astype(F32)
        r.part[src(k), :, quarter(t_x)] = other.astype(BF)
        back_x(k).start()

    def sum_x(k):
        back_x(k).wait_recv()
        mine = r.part[src(k), :, quarter(t)].astype(F32)
        mine = mine + r.from_core[k, half].astype(F32)
        return (mine + r.from_x[k].astype(F32)).astype(BF)

    def send_back(k):
        r.part[src(k), :, quarter(t)] = sum_x(k)
        back_ep(k).start()

    def grad_near(k):
        return remote(
            r.dg_send.at[dst(k)],
            r.dg_near.at[k],
            (r.send_dg.at[k], r.recv_dg.at[k]),
            (dst(k % near), t),
        )

    def grad_far(k):
        return remote(
            r.dg_send.at[dst(k)], r.dg_far.at[k], (r.send_dg.at[k], r.recv_dg.at[k]), (dst(k), t)
        )

    close = [k for k in range(n_ep) if k % near]
    far = list(range(near, n_ep, near))

    def grad_sum():
        for k in close:
            grad_near(k).wait_recv()
        for f in [0] + far:
            total = r.dg_send[dst(f)].astype(F32)
            for k in range(f + 1, f + near):
                total = total + r.dg_near[k].astype(F32)
            if f:
                r.dg_send[dst(f)] = total.astype(BF)
                grad_far(f).start()
            else:
                r.dg_in[...] = total[0]
                r.dg_out[...] = total[1]

    def gate_hop(k):
        return remote(
            r.gg_send.at[dst(k)], r.gg_back.at[me], (r.send_gg.at[k], r.recv_gg.at[k]), (dst(k), t)
        )

    own_rows, rank_r = r.in_own.shape
    span = n_ep // n_tp
    block_cols = width // n_ep

    def dense():
        in_whole = r.dense_all[:, :, 0].reshape(width, rank_r)
        out_whole = r.dense_all[:, :, 1].reshape(width, rank_r)
        pre = jnp.dot(r.tok[...], in_whole, preferred_element_type=F32)
        cob = jnp.dot(r.cot[...], out_whole, preferred_element_type=F32)
        gate = r.gate_row[...].astype(F32)
        gate = jnp.concatenate([gate[j : j + 1] for j in range(width // 128)], axis=1)
        r.gate_f32[...] = gate
        gate_wide = jnp.broadcast_to(gate, (16, width)).astype(BF)
        logit = lax.dot_general(
            r.tok[...], gate_wide, CONTRACT_COLS, preferred_element_type=F32
        )[:, :1]
        mix = jax.nn.sigmoid(logit)
        sig = jax.nn.sigmoid(pre)
        act = (pre * sig).astype(BF)
        dpre = (mix * cob * sig * (1.0 + pre * (1.0 - sig))).astype(BF)
        act_wide = act.astype(F32)
        dlogit = mix * (1.0 - mix) * jnp.sum(act_wide * cob, axis=1, keepdims=True)
        in_rows = r.dense_all[pl.ds(t * span, span), :, 0].reshape(cols, rank_r)
        dx = lax.dot_general(dpre, in_rows, CONTRACT_COLS, preferred_element_type=F32)
        r.dense_dx[...] = dx + dlogit * r.gate_f32[:, quarter(t)]
        lane = lax.broadcasted_iota(jnp.int32, (tok_dev, 128), 1)
        high = dlogit.astype(BF).astype(F32)
        low = dlogit - high
        pair = jnp.where(lane == 0, high, jnp.where(lane == 1, low, 0.0)).astype(BF)
        gate_sum = lax.dot_general(pair, r.tok[...], CONTRACT_ROWS, preferred_element_type=F32)
        gate_sum = gate_sum[0:1] + gate_sum[1:2]
        for e in range(n_ep):
            r.gg_send[e, :, :block_cols] = gate_sum[:, e * block_cols : (e + 1) * block_cols]
        mixed = (mix * act_wide).astype(BF)
        for a, (left, right) in enumerate(((r.tok, dpre), (r.cot, mixed))):
            r.grad_gate[:, :rank_r] = lax.dot_general(
                left[...], right, CONTRACT_ROWS, preferred_element_type=F32
            )
            for e in range(n_ep):
                start = pl.multiple_of((e * n_tp + t) * own_rows, own_rows)
                r.dg_send[e, a] = r.grad_gate[
                    pl.ds(start, own_rows), :rank_r
                ].astype(BF)
        r.gg_back[me] = r.gg_send[me]

        @pl.loop(1, n_ep)
        def _(k):
            gate_hop(k).start()

        for k in close:
            grad_near(k).start()

    @pl.loop(0, n_ep + 2)
    def _(n):
        @pl.when(n == 1)
        def _():
            sum_core(0)

        @pl.when(n == 3)
        def _():
            for f in far:
                shard_hop(0, f).wait_recv()
                shard_hop(1, f).start()
                shard_hop(2, f).start()
                for k in range(f + 1, f + near):
                    shard_hop(4, k).start()

        @pl.when((n >= 1) & (n < n_ep))
        def _():
            k = seq(n)
            c = k % near

            @pl.when(c > 0)
            def _():
                for a in range(2):
                    row_hop(a, 0, k).wait_recv()

                    @pl.when(k >= near)
                    def _():
                        row_hop(a, 1, k).start()

                    row_hop(a, 2, k).start()
                w_hop(k).wait_recv()

            @pl.when(c == 0)
            def _():
                i = src(k)
                s = i // near
                for kind in range(2):
                    info_hop(kind, k // near).wait_recv()
                place(s, r.pos, r.weight)
                pick, sent = pick_rows(r.pos, r.weight, me)
                r.w_all[i, :, :cap] = sent
                for a in range(2):

                    @pl.when((inner == 1) & (n == 1))
                    def _():
                        pass_on(a, 1)
                        pass_on(a, 3)

                    @pl.when(inner == 0)
                    def _():
                        raw_hop(a, s, False).wait_recv()

                    rows_all[a][i, :, quarter(t)] = picked(pick, raw[a][s])
                    pick_close(a, k, r.pos, lambda: raw[a][s])
                    row_hop(a, 1, k).start()
                    row_hop(a, 2, k).start()
                    send_close(a, k)

                weigh_close(k, r.pos, r.weight)

        @pl.when(n >= 4)
        def _():
            sum_core(seq(n - 3))

        @pl.when(n == 3)
        def _():
            r.rows_back[me] = sum_x(0)

        @pl.when(n >= 5)
        def _():
            send_back(seq(n - 4))

        @pl.when((n == 0) | (n >= 3))
        def _():
            k = seq(jnp.where(n == 0, 0, n - 2))

            @pl.when(n >= 3)
            def _():
                for a in range(2):
                    for kind in (2, 3):
                        row_hop(a, kind, k).wait_recv()

            run(k)

        @pl.when(n == 0)
        def _():
            @pl.loop(0, n_ep)
            def _(e):
                pick, _ = pick_rows(r.own_pos, r.own_weight, e)
                r.picks[e] = pick

        @pl.when(n == 4)
        def _():
            for f in [0] + far:
                shard_hop(1, f).wait_recv()
                shard_hop(3, f).start()
                for k in range(f + 1, f + near):
                    shard_hop(5, k).start()

        @pl.when(n == 5)
        def _():
            for k in close:
                shard_hop(4, k).wait_recv()
                shard_hop(2, k).start()
                shard_hop(5, k).wait_recv()
                shard_hop(3, k).start()

        @pl.when((n >= 2) & (n < n_ep + 1))
        def _():
            k = seq(n - 1)
            for a in range(2):
                row_hop(a, 1, k).wait_recv()
                row_hop(a, 3, k).start()

        @pl.when(n == 7)
        def _():
            grad_sum()

        @pl.when((inner == 1) & (n == near + 1))
        def _():
            for a in range(2):
                pass_on(a, 2)

        @pl.when(n == 6)
        def _():
            @pl.loop(0, n_ep)
            def _(k):
                for kind in (2, 3):
                    shard_hop(kind, k).wait_recv()

            dense()

    rows = n_ep * cap
    tiles = width // cols

    def tile(kind, j):
        if kind == 0:
            r.grad_down[:, quarter(j)] = lax.dot_general(
                r.act[...].reshape(rows, -1),
                r.dy_all.reshape(rows, width)[:, quarter(j)],
                CONTRACT_ROWS,
                preferred_element_type=F32,
            )
            return
        out, right = ((r.grad_gate, r.d_gate), (r.grad_up, r.d_up))[kind - 1]
        out[quarter(j), :] = lax.dot_general(
            r.x_all.reshape(rows, width)[:, quarter(j)],
            right[...].reshape(rows, -1),
            CONTRACT_ROWS,
            preferred_element_type=F32,
        )

    def weight_core():
        return remote(r.w_part, r.w_from.at[0], (r.send_wt.at[0], r.recv_wt.at[0]), core_peer)

    def weight_x():
        return remote(r.w_half, r.w_from.at[1], (r.send_wt.at[1], r.recv_wt.at[1]), x_peer)

    def weight_ep(k):
        return remote(
            r.w_sum.at[src(k)], r.w_back.at[me], (r.send_we.at[k], r.recv_we.at[k]), (src(k), t)
        )

    weight_core().start()
    tile(0, 0)
    sum_core(seq(n_ep - 1))
    weight_core().wait_recv()
    r.w_half[...] = r.w_part[...] + r.w_from[0]
    send_back(seq(n_ep - 2))
    weight_x().start()
    for j in range(1, tiles):
        tile(0, j)
    weight_x().wait_recv()
    r.w_sum[...] = r.w_half[...] + r.w_from[1]
    send_back(seq(n_ep - 1))
    r.w_back[me] = r.w_sum[me]

    @pl.loop(1, n_ep)
    def _(k):
        weight_ep(k).start()

    for kind in (1, 2):
        for j in range(tiles):
            tile(kind, j)

    @pl.loop(1, n_ep)
    def _(k):
        gate_hop(k).wait_recv()

    for f in far:
        grad_far(f).wait_recv()
        r.dg_in[...] += r.dg_far[f, 0].astype(F32)
        r.dg_out[...] += r.dg_far[f, 1].astype(F32)
    gate_total = jnp.zeros(r.gg_back.shape[1:], F32)
    for e in range(n_ep):
        gate_total = gate_total + r.gg_back[e]
    block = block_cols // n_tp
    r.gg_out[...] = sum(
        jnp.where(t == q, gate_total[:, q * block : (q + 1) * block], 0.0) for q in range(n_tp)
    )

    @pl.loop(1, n_ep)
    def _(k):
        weight_ep(k).wait_recv()
        back_ep(k).wait_recv()

    picks = r.picks[...].reshape(rows, tok_dev)
    moved = lax.dot_general(
        picks,
        r.rows_back[...].reshape(rows, cols),
        CONTRACT_ROWS,
        preferred_element_type=F32,
    )
    r.grad_tokens[...] = (r.dense_dx[...] + moved).astype(BF)
    found = [jnp.zeros((1, tok_dev), F32) for _ in range(top_k)]
    for e in range(n_ep):
        row = r.w_back[e]
        row = jnp.broadcast_to(row, (16, lanes)).astype(BF)[:, :cap]
        spread = jnp.dot(row, r.picks[e], preferred_element_type=F32)[0:1]
        for k in range(top_k):
            found[k] = found[k] + jnp.where(r.ids[k : k + 1, :] == e, spread, 0.0)
    for k in range(top_k):
        r.grad_route[k : k + 1, :] = found[k].astype(BF)

    for f in [0] + far:
        shard_hop(1, f).wait_send()
    for f in far:
        shard_hop(0, f).wait_send()
        grad_far(f).wait_send()
    for f in range(1, planes):
        for kind in range(2):
            info_hop(kind, f).wait_send()
    for a in range(2):
        each_own(a, lambda c: c.wait_send())
        for s in range(planes):
            each_raw(a, s, lambda c: c.wait_send())
    for k in close:
        w_hop(k).wait_send()
        for a in range(2):
            row_hop(a, 0, k).wait_send()
        shard_hop(4, k).wait_send()
        shard_hop(5, k).wait_send()
        grad_near(k).wait_send()

    @pl.loop(0, n_ep)
    def _(k):
        for kind in (2, 3):
            shard_hop(kind, k).wait_send()
        for h in range(2):
            back_core(k, h).wait_send()
        back_x(k).wait_send()

    @pl.loop(1, n_ep)
    def _(k):
        for a in range(2):
            for kind in range(1, 4):
                row_hop(a, kind, k).wait_send()
        back_ep(k).wait_send()
        weight_ep(k).wait_send()
        gate_hop(k).wait_send()

    weight_core().wait_send()
    weight_x().wait_send()


def store_kernel(count, *refs):
    copies = [
        pltpu.make_async_copy(refs[n], refs[count + n], refs[2 * count].at[n])
        for n in range(count)
    ]
    for c in copies:
        c.start()
    for c in copies:
        c.wait()


def store(arrays):
    return pl.pallas_call(
        functools.partial(store_kernel, len(arrays)),
        out_shape=tuple(jax.ShapeDtypeStruct(a.shape, a.dtype) for a in arrays),
        in_specs=[VMEM] * len(arrays),
        out_specs=(ANY,) * len(arrays),
        scratch_shapes=[pltpu.SemaphoreType.DMA((len(arrays),))],
        compiler_params=pltpu.CompilerParams(vmem_limit_bytes=16 * 1024 * 1024),
        name="store",
    )(*arrays)


def shards(
    tokens,
    cotangent,
    route_ids,
    route_weights,
    w_gate,
    w_up,
    w_down,
    dense_in,
    dense_out,
    dense_gate,
):
    n_ep = lax.axis_size("ep")
    n_tp = lax.axis_size("tp")
    tok_dev, width = tokens.shape
    top_k = route_ids.shape[1]
    cols = width // n_tp
    near = n_ep // 4
    cap = 2 * tok_dev * top_k // n_ep
    lanes = -(-cap // 128) * 128
    hidden = w_gate.shape[2]
    own_rows, rank_r = dense_in.shape
    gate_lanes = -(-(width // n_ep) // 128) * 128
    dma = pltpu.SemaphoreType.DMA
    args = dict(
        ids=(route_ids.T, VMEM),
        route=(route_weights.T, VMEM),
        gate_row=(dense_gate.reshape(-1, 128), VMEM),
        tokens=(tokens, ANY),
        cotangent=(cotangent, ANY),
        in_own=(dense_in, ANY),
        out_own=(dense_out, ANY),
        w_gate=(w_gate[0], ANY),
        w_up=(w_up[0], ANY),
        w_down=(w_down[0], ANY),
    )
    outs = dict(
        grad_tokens=((tok_dev, cols), BF),
        grad_route=((top_k, tok_dev), BF),
        grad_gate=((width, hidden), F32),
        grad_up=((width, hidden), F32),
        grad_down=((hidden, width), F32),
        dg_in=((own_rows, rank_r), F32),
        dg_out=((own_rows, rank_r), F32),
        gg_out=((1, width // (n_ep * n_tp)), F32),
    )
    scratch = dict(
        tok=((tok_dev, width), BF),
        cot=((tok_dev, width), BF),
        gate_w=((width, hidden), BF),
        up_w=((width, hidden), BF),
        down_w=((hidden, width), BF),
        own_pos=((max(16, n_ep), tok_dev), F32),
        own_weight=((max(16, n_ep), tok_dev), F32),
        pos=((max(16, n_ep), tok_dev), F32),
        weight=((max(16, n_ep), tok_dev), F32),
        below=((tok_dev, tok_dev), BF),
        ids_all=((4, top_k, tok_dev), jnp.int32),
        route_all=((4, top_k, tok_dev), F32),
        x_extra=((near, cap, cols), BF),
        dy_extra=((near, cap, cols), BF),
        x_raw=((4, tok_dev, cols), BF),
        dy_raw=((4, tok_dev, cols), BF),
        picks=((n_ep, cap, tok_dev), BF),
        w_send=((n_ep, 1, lanes), F32),
        w_all=((n_ep, 1, lanes), F32),
        x_send=((n_ep, cap, cols), BF),
        dy_send=((n_ep, cap, cols), BF),
        x_all=((n_ep, cap, width), BF),
        dy_all=((n_ep, cap, width), BF),
        act=((n_ep, cap, hidden), BF),
        d_gate=((n_ep, cap, hidden), BF),
        d_up=((n_ep, cap, hidden), BF),
        part=((n_ep, cap, width), BF),
        w_part=((n_ep, 1, lanes), F32),
        from_core=((n_ep, 2, cap, cols), BF),
        from_x=((n_ep, cap, cols), BF),
        rows_back=((n_ep, cap, cols), BF),
        dense_all=((n_ep, n_tp, 2, own_rows, rank_r), BF),
        dense_dx=((tok_dev, cols), F32),
        gate_f32=((1, width), F32),
        dg_send=((n_ep, 2, own_rows, rank_r), BF),
        dg_near=((n_ep, 2, own_rows, rank_r), BF),
        dg_far=((n_ep, 2, own_rows, rank_r), BF),
        gg_send=((n_ep, 1, gate_lanes), F32),
        gg_back=((n_ep, 1, gate_lanes), F32),
        w_from=((2, n_ep, 1, lanes), F32),
        w_half=((n_ep, 1, lanes), F32),
        w_sum=((n_ep, 1, lanes), F32),
        w_back=((n_ep, 1, lanes), F32),
    )
    sems = dict(
        load_sem=(7,),
        send_info=(2, 4),
        recv_info=(2, 4),
        send_raw=(2, 2, 4),
        recv_raw=(2, 4),
        send_rows=(2, 4, n_ep),
        recv_rows=(2, 4, n_ep),
        send_shard=(6, n_ep),
        recv_shard=(6, n_ep),
        send_w=(n_ep,),
        recv_w=(n_ep,),
        send_bc=(n_ep, 2),
        recv_bc=(n_ep, 2),
        send_bx=(n_ep,),
        recv_bx=(n_ep,),
        send_be=(n_ep,),
        recv_be=(n_ep,),
        send_dg=(n_ep,),
        recv_dg=(n_ep,),
        send_gg=(n_ep,),
        recv_gg=(n_ep,),
        send_wt=(2,),
        recv_wt=(2,),
        send_we=(n_ep,),
        recv_we=(n_ep,),
    )
    names = list(args) + list(outs) + list(scratch) + list(sems)
    results = pl.pallas_call(
        functools.partial(layer_kernel, n_ep, n_tp, names),
        out_shape=tuple(pltpu.VMEM(s, d) for s, d in outs.values()),
        in_specs=[spec for _, spec in args.values()],
        out_specs=(VMEM,) * len(outs),
        scratch_shapes=[pltpu.VMEM(s, d) for s, d in scratch.values()]
        + [dma(s) for s in sems.values()],
        compiler_params=pltpu.CompilerParams(
            collective_id=0, has_side_effects=True, vmem_limit_bytes=48 * 1024 * 1024
        ),
        name="layer",
    )(*(a for a, _ in args.values()))
    grad_tokens, grad_route, grad_gate, grad_up, grad_down, dg_in, dg_out, gg_out = store(results)
    return (
        grad_tokens,
        grad_route.T,
        grad_gate[None],
        grad_up[None],
        grad_down[None],
        dg_in,
        dg_out,
        gg_out[0],
    )


def solution(mesh):
    placed = (
        P("ep", None),
        P("ep", None),
        P("ep", None),
        P("ep", None),
        P("ep", None, "tp"),
        P("ep", None, "tp"),
        P("ep", "tp", None),
        P(("ep", "tp"), None),
        P(("ep", "tp"), None),
        P(),
    )
    return jax.shard_map(
        shards,
        mesh=mesh,
        in_specs=placed,
        out_specs=(
            P("ep", "tp"),
            P("ep", None),
            P("ep", None, "tp"),
            P("ep", None, "tp"),
            P("ep", "tp", None),
            P(("ep", "tp"), None),
            P(("ep", "tp"), None),
            P(("ep", "tp")),
        ),
        check_vma=False,
    )
```

time: 149 us -> 125 us (0.84)
  local copies, waits for them, and re-layouts: 17.6 us -> 0 us
  Pallas kernels: 130 us -> 124 us
    unnamed x9 -> x0, local copies, waits for them, and re-layouts: 13.5 us -> none
    pallas_call x1, Pallas kernels: 130 us -> 119 us  [shards(): pl.pallas_call(functools.partial(layer_kernel, n_ep, n_tp, names), out_sh...]
    pallas_call x0 -> x1, Pallas kernels: none -> 4.85 us  [store(): pl.pallas_call(functools.partial(store_kernel, len(arrays)), out_shape=tu...]
    squeeze x1 -> x0, local copies, waits for them, and re-layouts: 1.53 us -> none  [shards(): dg_out[1]]
where the time goes in v2:
time: 125 us
  Pallas kernels  124 us (99%)
    pallas_call x1, Pallas kernels, shards(): pl.pallas_call(functools.partial(layer_kernel, n_ep, n_tp, names), out_sh...  119 us
    pallas_call x1, Pallas kernels, store(): pl.pallas_call(functools.partial(store_kernel, len(arrays)), out_shape=tu...  4.85 us

profile of v2, /device:TPU:0, one launch (start us, length us, event | category | flops | bytes accessed | tf_op | source)
XLA Modules:
  0.0 124.6 jit_solution(4805542940361831195)
XLA Ops:
  0.6 119.0 %layer.1 = (bf16[320,512]{1,0:T(8,128)(2,1)S(1)}, bf16[2,320]{1,0:T(2,128)(2,1)S(1)}, f32[2048,512]{1,0:T(8,128)S(1)}, f32[2048,512]{1,0:T(8,128)S(1)}, f32[512,...) custom-call(s32[2,320]{1,0:T(2,128)} %bitcast.15, ...), custom_call_target="tpu_custom_call" | custom-call | tf_op jit(solution)/shard_map/layer/pallas_call | solution.py:863
  119.6 4.8 %store.1 = (bf16[320,512]{1,0:T(8,128)(2,1)}, bf16[2,320]{1,0:T(2,128)(2,1)}, f32[2048,512]{1,0:T(8,128)}, f32[2048,512]{1,0:T(8,128)}, f32[512,2048]{1,0:T(8,12...) custom-call(bf16[320,512]{1,0:T(8,128)(2,1)S(1)} %get-tuple-element.24.refs_0_, ...), custom_call_target="tpu_custom_call" | custom-call | tf_op jit(solution)/shard_map/store/pallas_call | solution.py:733

commit v3 on v2

--- a/solution.py
+++ b/solution.py
@@ -51,7 +51,7 @@
     def seq(n):
         p = n + near - 1
         f = p // near
-        k = jnp.where((f >= 2) & (inner == 1), (5 - f) * near + p % near, p)
+        k = jnp.where(inner == 1, ((f + 1) % 3 + 1) * near + p % near, p)
         k = jnp.where(n > n_ep - near, n - (n_ep - near), k)
         return jnp.where(n == 0, 0, k)
 
@@ -521,9 +521,9 @@
         def _():
             r.rows_back[me] = sum_x(0)
 
-        @pl.when(n >= 5)
-        def _():
-            send_back(seq(n - 4))
+        @pl.when(n >= 6)
+        def _():
+            send_back(seq(n - 5))
 
         @pl.when((n == 0) | (n >= 3))
         def _():
@@ -544,7 +544,7 @@
                 pick, _ = pick_rows(r.own_pos, r.own_weight, e)
                 r.picks[e] = pick
 
-        @pl.when(n == 4)
+        @pl.when(n == 3)
         def _():
             for f in [0] + far:
                 shard_hop(1, f).wait_recv()
@@ -552,7 +552,7 @@
                 for k in range(f + 1, f + near):
                     shard_hop(5, k).start()
 
-        @pl.when(n == 5)
+        @pl.when(n == 4)
         def _():
             for k in close:
                 shard_hop(4, k).wait_recv()
@@ -567,7 +567,7 @@
                 row_hop(a, 1, k).wait_recv()
                 row_hop(a, 3, k).start()
 
-        @pl.when(n == 7)
+        @pl.when(n == 6)
         def _():
             grad_sum()
 
@@ -576,7 +576,7 @@
             for a in range(2):
                 pass_on(a, 2)
 
-        @pl.when(n == 6)
+        @pl.when(n == 5)
         def _():
             @pl.loop(0, n_ep)
             def _(k):
@@ -617,6 +617,7 @@
         )
 
     weight_core().start()
+    send_back(seq(n_ep - 3))
     tile(0, 0)
     sum_core(seq(n_ep - 1))
     weight_core().wait_recv()

time: 125 us -> 115 us (0.920)
  Pallas kernels: 124 us -> 114 us
    pallas_call x1, Pallas kernels: 119 us -> 109 us  [shards(): pl.pallas_call(functools.partial(layer_kernel, n_ep, n_tp, names), out_sh...]
where the time goes in v3:
time: 115 us
  Pallas kernels  114 us (99%)
    pallas_call x1, Pallas kernels, shards(): pl.pallas_call(functools.partial(layer_kernel, n_ep, n_tp, names), out_sh...  109 us
    pallas_call x1, Pallas kernels, store(): pl.pallas_call(functools.partial(store_kernel, len(arrays)), out_shape=tu...  4.85 us

profile of v3, /device:TPU:0, one launch (start us, length us, event | category | flops | bytes accessed | tf_op | source)
XLA Modules:
  0.0 114.8 jit_solution(16666669148137544172)
XLA Ops:
  0.6 109.2 %layer.1 = (bf16[320,512]{1,0:T(8,128)(2,1)S(1)}, bf16[2,320]{1,0:T(2,128)(2,1)S(1)}, f32[2048,512]{1,0:T(8,128)S(1)}, f32[2048,512]{1,0:T(8,128)S(1)}, f32[512,...) custom-call(s32[2,320]{1,0:T(2,128)} %bitcast.15, ...), custom_call_target="tpu_custom_call" | custom-call | tf_op jit(solution)/shard_map/layer/pallas_call | solution.py:864
  109.8 4.8 %store.1 = (bf16[320,512]{1,0:T(8,128)(2,1)}, bf16[2,320]{1,0:T(2,128)(2,1)}, f32[2048,512]{1,0:T(8,128)}, f32[2048,512]{1,0:T(8,128)}, f32[512,2048]{1,0:T(8,12...) custom-call(bf16[320,512]{1,0:T(8,128)(2,1)S(1)} %get-tuple-element.24.refs_0_, ...), custom_call_target="tpu_custom_call" | custom-call | tf_op jit(solution)/shard_map/store/pallas_call | solution.py:734
